TPU v7x, 32 devices: a whole 2x2x4 slice. The times are simulated.
32 devices in a mesh: sp: 16 (over z, y, x), tp: 2 (over core).
Axes of the slice: x: 2, y: 2, z: 4, core: 2. Of those that a mesh axis runs over, the one named last changes fastest.
Arguments:
- prompt: bfloat16 [2, 3072, 4096], P(None, 'sp'), as said below
- w_key: bfloat16 [4096, 2048], P('sp', 'tp'), may hold values from -0.09375 to 0.09375
- w_value: bfloat16 [4096, 4096], P('sp', 'tp'), may hold values from -0.09375 to 0.09375
- w_igate: bfloat16 [4096, 8], replicated, may hold values from -0.09375 to 0.09375
- w_fgate: bfloat16 [4096, 8], replicated, may hold values from -0.09375 to 0.09375
- input_bias: float32 [8], replicated, may hold values from -1 to 120
- forget_bias: float32 [8], replicated, may hold values from 4 to 20
- new_query: bfloat16 [2, 8, 256], P(None, 'tp'), may hold values from -6 to 6
- new_key: bfloat16 [2, 8, 256], P(None, 'tp'), may hold values from -6 to 6
- new_value: bfloat16 [2, 8, 512], P(None, 'tp'), may hold values from -6 to 6
- new_gates: float32 [2, 2, 8], P(None, None, 'tp'), may hold values from 2 to 9
Outputs:
- cache_memory: bfloat16 [2, 8, 256, 512], P(None, 'tp', 'sp')
- cache_norm: float32 [2, 8, 256], P(None, 'tp', 'sp')
- cache_max: float32 [2, 8], P(None, 'tp')
- first_read: bfloat16 [2, 8, 512], P(None, 'tp')
Inputs may be any that keep to these rules, and one draw needn't show every extreme that they name: `prompt`: Real-valued features, each entry drawn independently; their magnitude differs from one block of 192 positions to the next.
All inputs are finite; a program needn't handle non-finite values.
Results may differ from a plain program's by a relative error of at most 0.019.
Values may be sent and summed in bfloat16 or wider, within the bound.
A program may use at most 64 MiB of HBM per device.

v0:
```python
import functools
import jax
import jax.numpy as jnp
from jax import lax
from jax.experimental import pallas as pl
from jax.experimental.pallas import tpu as pltpu
from jax.sharding import PartitionSpec as P

CHUNKS = 8
PER = CHUNKS // 4
HIGH = lax.Precision.HIGHEST


def flip(bit, change):
    return bit + change - 2 * bit * change


def log_sigmoid(v):
    return jnp.minimum(v, 0.0) - jnp.log1p(jnp.exp(-jnp.abs(v)))


def kernel(
    prompt,
    w_key,
    w_value,
    w_igate,
    w_fgate,
    input_bias,
    forget_bias,
    new_query,
    new_key,
    new_value,
    new_gates,
    memory_out,
    norm_out,
    max_out,
    read_out,
    xb,
    wk,
    wv,
    w_gate,
    key_acc,
    value_acc,
    decay,
    vals,
    weight,
    stat,
    state,
    aux,
    yin,
    yaux,
    total_state,
    total_aux,
    rmem,
    raux,
    local_sem,
    x_send,
    x_recv,
    d_send,
    d_recv,
    wk_send,
    wk_recv,
    wv_send,
    wv_recv,
    s_send,
    s_recv,
    y_send,
    y_recv,
    m_send,
    m_recv,
    a_send,
    a_recv,
):
    count = lax.axis_size("sp")
    me = lax.axis_index("sp")
    core = lax.axis_index("tp")
    seqs, span, width = prompt.shape
    depth = w_key.shape[0]
    heads = new_query.shape[1]
    dk = new_query.shape[2]
    dv = new_value.shape[2]
    total_heads = input_bias.shape[1]
    key_scale = dk ** (-0.5)
    cut = width // CHUNKS
    rows_out = dk // count
    zh, zl, y, x = me // 8, (me // 4) % 2, (me // 2) % 2, me % 2
    mine = zl * 2 + x

    def place(dh, dy, dz, dx):
        return flip(zh, dh) * 8 + flip(zl, dz) * 4 + flip(y, dy) * 2 + flip(x, dx)

    def remote(src, dst, send, recv, sp, tp):
        return pltpu.make_async_remote_copy(
            src_ref=src,
            dst_ref=dst,
            send_sem=send,
            recv_sem=recv,
            device_id=(sp, tp),
            device_id_type=pl.DeviceIdType.MESH,
        )

    ring = [(0, 0), (0, 1), (1, 0), (1, 1)]
    clique = [(0, 0), (0, 1), (1, 0), (1, 1)]
    sent = []

    def go(copy):
        copy.start()
        sent.append(copy)

    barrier = pltpu.get_barrier_semaphore()
    for off in range(1, count):
        pl.semaphore_signal(
            barrier,
            inc=1,
            device_id=((me + off) % count, core),
            device_id_type=pl.DeviceIdType.MESH,
        )
    pl.semaphore_signal(
        barrier, inc=1, device_id=(me, 1 - core), device_id_type=pl.DeviceIdType.MESH
    )

    def w_rows(slot):
        q, r = slot // 4, slot % 4
        src = place(*clique[q], *ring[r])
        return pl.ds(pl.multiple_of(src * depth, depth), depth)

    own_x = []
    for s in range(seqs):
        c = pltpu.make_async_copy(
            prompt.at[s], xb.at[0, pl.ds(s * span, span)], local_sem.at[s]
        )
        c.start()
        own_x.append(c)
    kcols = pl.ds(pl.multiple_of(mine * dk, dk), dk)
    vcols = pl.ds(pl.multiple_of(mine * dv, dv), dv)
    own_rows = w_rows(0)
    own_k = pltpu.make_async_copy(w_key.at[:, kcols], wk.at[own_rows], local_sem.at[2])
    own_v = pltpu.make_async_copy(w_value.at[:, vcols], wv.at[own_rows], local_sem.at[3])
    own_k.start()
    own_v.start()
    pl.semaphore_wait(barrier, count)

    for r in (1, 2, 3):
        dz, dx = ring[r]
        peer = place(0, 0, dz, dx)
        theirs = flip(zl, dz) * 2 + flip(x, dx)
        kc = pl.ds(pl.multiple_of(theirs * dk, dk), dk)
        vc = pl.ds(pl.multiple_of(theirs * dv, dv), dv)
        go(remote(w_key.at[:, kc], wk.at[own_rows], wk_send.at[r], wk_recv.at[r], peer, core))
        go(remote(w_value.at[:, vc], wv.at[own_rows], wv_send.at[r], wv_recv.at[r], peer, core))

    def w_relay(slot, to, tag):
        rows = w_rows(slot)
        q = slot // 4
        there = (q + to[0] * 2 + to[1]) * 4 + slot % 4
        peer = place(to[0], to[1], 0, 0)
        go(remote(wk.at[rows], wk.at[rows], wk_send.at[tag], wk_recv.at[there], peer, core))
        go(remote(wv.at[rows], wv.at[rows], wv_send.at[tag], wv_recv.at[there], peer, core))

    def w_wait(slot):
        rows = w_rows(slot)
        pltpu.make_async_copy(wk.at[rows], wk.at[rows], wk_recv.at[slot]).wait()
        pltpu.make_async_copy(wv.at[rows], wv.at[rows], wv_recv.at[slot]).wait()

    def x_part(slot, seq_rows, k):
        return xb.at[slot, seq_rows, pl.ds(k * cut, cut)]

    my_rows = pl.ds(pl.multiple_of(core * span, span), span)
    other_rows = pl.ds(pl.multiple_of((1 - core) * span, span), span)
    to_x, to_z = place(0, 0, 0, 1), place(0, 0, 1, 0)

    def x_send_own(slot, k, peer):
        go(
            remote(
                prompt.at[core, :, pl.ds(k * cut, cut)],
                x_part(slot, my_rows, k),
                x_send.at[slot, k],
                x_recv.at[slot, k],
                peer,
                core,
            )
        )

    def x_wait(slot, k):
        part = x_part(slot, my_rows, k)
        pltpu.make_async_copy(part, part, x_recv.at[slot, k]).wait()

    def x_across(slot, k):
        part = x_part(slot, my_rows, k)
        go(remote(part, part, d_send.at[slot, k], d_recv.at[slot, k], me, 1 - core))

    def d_wait(slot, k):
        part = x_part(slot, other_rows, k)
        pltpu.make_async_copy(part, part, d_recv.at[slot, k]).wait()

    for k in range(PER):
        x_send_own(2, k, to_z)
    for k in range(CHUNKS):
        x_send_own(1, k, to_x)
    own_k.wait()
    own_v.wait()
    w_relay(0, (1, 0), 4)
    w_relay(0, (0, 1), 8)
    for r in (1, 2, 3):
        w_wait(r)
        w_relay(r, (1, 0), 4 + r)
        w_relay(r, (0, 1), 8 + r)
        for k in range(PER):
            x_send_own(2, r * PER + k, to_z)
    for c in own_x:
        c.wait()

    lane = lax.broadcasted_iota(jnp.int32, (seqs * span, 2 * total_heads), 1)
    head = core * heads + mine
    w_gate[...] = jnp.concatenate([w_igate[...], w_fgate[...]], axis=0)
    head_lane = lax.broadcasted_iota(jnp.int32, (1, total_heads), 1) == head
    bias_in = jnp.sum(jnp.where(head_lane, input_bias[...], 0.0), axis=1, keepdims=True)
    bias_f = jnp.sum(jnp.where(head_lane, forget_bias[...], 0.0), axis=1, keepdims=True)
    at_t = lax.broadcasted_iota(jnp.int32, (span, span), 0)
    at_u = lax.broadcasted_iota(jnp.int32, (span, span), 1)
    after = (at_u > at_t).astype(jnp.float32)
    stat_row = lax.broadcasted_iota(jnp.int32, (8, 128), 0)
    stat_lane = lax.broadcasted_iota(jnp.int32, (8, 128), 1)

    def gates(r, table):
        both = lax.dot_general(
            xb[r],
            w_gate[...],
            (((1,), (1,)), ((), ())),
            preferred_element_type=jnp.float32,
        )
        gate_in = bias_in + jnp.sum(jnp.where(lane == head, both, 0.0), axis=1, keepdims=True)
        gate_f = bias_f + jnp.sum(
            jnp.where(lane == total_heads + head, both, 0.0), axis=1, keepdims=True
        )
        forget = log_sigmoid(gate_f)
        for s in range(seqs):
            part = forget[s * span : (s + 1) * span]
            wide = jnp.broadcast_to(part, (span, 128))
            later = jnp.dot(after, wide, precision=HIGH, preferred_element_type=jnp.float32)
            level = later[:, 0:1] + gate_in[s * span : (s + 1) * span]
            top = jnp.max(level, axis=0, keepdims=True)
            total = jnp.sum(part, axis=0, keepdims=True)
            weight[r, s * span : (s + 1) * span] = jnp.broadcast_to(
                jnp.exp(level - top) * key_scale, (span, 128)
            )
            hit = stat_row == r * seqs + s
            table = jnp.where(hit & (stat_lane == 0), total, table)
            table = jnp.where(hit & (stat_lane == 1), top, table)
        return table

    def project(r, slots, first):
        def step(i, carry):
            keys = values = None
            for off in range(2):
                rows = slots(2 * i + off)
                tokens = xb[r, :, rows]
                k_part = jnp.dot(tokens, wk[rows], preferred_element_type=jnp.float32)
                v_part = jnp.dot(tokens, wv[rows], preferred_element_type=jnp.float32)
                keys = k_part if keys is None else keys + k_part
                values = v_part if values is None else values + v_part
            key_acc[r] += keys
            value_acc[r] += values
            return carry

        if first:
            key_acc[r] = jnp.zeros((seqs * span, dk), jnp.float32)
            value_acc[r] = jnp.zeros((seqs * span, dv), jnp.float32)
        return step

    def source_rows(q):
        def rows(r):
            dh, dy = clique[q]
            dz, dx = r // 2, r % 2
            src = place(dh, dy, dz, dx)
            return pl.ds(pl.multiple_of(src * depth, depth), depth)

        return rows

    def group(r, q, first=False):
        lax.fori_loop(0, 2, project(r, source_rows(q), first), 0)

    def finish(r):
        keys = key_acc[r].astype(jnp.bfloat16).astype(jnp.float32)
        decay[r] = (weight[r, :, 0:1] * keys).astype(jnp.bfloat16)
        vals[r] = value_acc[r].astype(jnp.bfloat16)

    table = gates(0, jnp.zeros((8, 128), jnp.float32))
    group(0, 0, True)
    for k in range(4):
        for c in range(k * PER, (k + 1) * PER):
            x_wait(2, c)
            go(
                remote(
                    x_part(2, my_rows, c),
                    x_part(3, my_rows, c),
                    x_send.at[3, c],
                    x_recv.at[3, c],
                    to_x,
                    core,
                )
            )
            x_across(2, c)
        w_wait(8 + k)
        w_relay(8 + k, (0, 1), 12 + k)
        if k == 1:
            for c in range(CHUNKS):
                x_wait(1, c)
                x_across(1, c)
            for slot in range(4, 8):
                w_wait(slot)
            group(0, 1)
        if k == 2:
            for c in range(CHUNKS):
                d_wait(1, c)
            table = gates(1, table)
            group(1, 0, True)
            group(1, 1)
    group(0, 2)
    group(1, 2)
    for c in range(CHUNKS // 2):
        x_wait(3, c)
        x_across(3, c)
    for c in range(CHUNKS):
        d_wait(2, c)
    table = gates(2, table)
    for q in range(3):
        group(2, q, q == 0)
    for c in range(CHUNKS // 2, CHUNKS):
        x_wait(3, c)
        x_across(3, c)
    for slot in range(12, 16):
        w_wait(slot)
    for c in range(CHUNKS):
        d_wait(3, c)
    table = gates(3, table)
    stat[0] = table
    for r in range(3):
        group(r, 3)
        finish(r)
    for q in (1, 2, 3):
        dh, dy = clique[q]
        go(
            remote(
                stat.at[0], stat.at[q], s_send.at[q], s_recv.at[q], place(dh, dy, 0, 0), core
            )
        )
    for q in range(4):
        group(3, q, q == 0)
    finish(3)
    for q in (1, 2, 3):
        pltpu.make_async_copy(stat.at[q], stat.at[q], s_recv.at[q]).wait()

    stats = jnp.concatenate([stat[q] for q in range(4)], axis=0)

    def spot(dim):
        n = lax.broadcasted_iota(jnp.int32, (32, 32), dim)
        dh, dy, dz, dx = n // 16, (n // 8) % 2, (n // 4) % 2, (n // 2) % 2
        where = flip(zh, dh) * 8 + flip(zl, dz) * 4 + flip(y, dy) * 2 + flip(x, dx)
        return where, n % 2

    (pos_a, seq_a), (pos_b, seq_b) = spot(0), spot(1)
    later_mask = ((pos_b > pos_a) & (seq_a == seq_b)).astype(jnp.float32)
    later = jnp.dot(later_mask, stats, precision=HIGH, preferred_element_type=jnp.float32)
    lift = later[:, 0:1] + stats[:, 1:2]
    parity = lax.broadcasted_iota(jnp.int32, (32, 1), 0) % 2
    highest = [
        jnp.max(jnp.where(parity == s, lift, -jnp.inf), axis=0, keepdims=True)
        for s in range(seqs)
    ]
    factor = jnp.exp(lift - jnp.where(parity == 0, highest[0], highest[1]))

    pick = lax.broadcasted_iota(jnp.int32, (heads, dk), 0) == mine
    ones = jnp.ones((8, span), jnp.bfloat16)
    aux_row = lax.broadcasted_iota(jnp.int32, (1, 128), 1)
    tail = jnp.zeros((1, 128), jnp.float32)

    to_y = place(0, 1, 0, 0)
    half = count // 2
    spot8 = (zh * 2 + zl) * 2 + x

    def cut_rows(spot):
        return pl.ds(pl.multiple_of(spot * rows_out, rows_out), rows_out)

    for s in range(seqs):
        sums = jnp.zeros((dk, dv), jnp.float32)
        norms = jnp.zeros((8, dk), jnp.float32)
        for r in range(4):
            d = decay[r, s * span : (s + 1) * span]
            v = vals[r, s * span : (s + 1) * span]
            f = factor[r * seqs + s : r * seqs + s + 1, 0:1]
            sums = sums + f * lax.dot_general(
                d, v, (((0,), (0,)), ((), ())), preferred_element_type=jnp.float32
            )
            norms = norms + f * jnp.dot(ones, d, preferred_element_type=jnp.float32)
        for block in range(count // 2):
            rows = sums[block * 2 * rows_out : (block + 1) * 2 * rows_out]
            low = (block // 2) * 2 * rows_out
            state[s, block % 2, low : low + 2 * rows_out] = rows.astype(jnp.bfloat16)
        query = jnp.sum(
            jnp.where(pick, new_query[s].astype(jnp.float32), 0.0), axis=0, keepdims=True
        )
        seen = jnp.dot(
            jnp.broadcast_to(query, (8, dk)),
            sums,
            precision=HIGH,
            preferred_element_type=jnp.float32,
        )
        for k in range(dv // 128):
            aux[s * 4 + k : s * 4 + k + 1] = seen[0:1, k * 128 : (k + 1) * 128]
        for k in range(dk // 128):
            row = 8 + s * 2 + k
            aux[row : row + 1] = norms[0:1, k * 128 : (k + 1) * 128]
        dot_norm = jnp.sum(query * norms[0:1], axis=1, keepdims=True)
        tail = jnp.where(aux_row == s, highest[s], tail)
        tail = jnp.where(aux_row == 2 + s, dot_norm, tail)
        go(
            remote(state.at[s, 1 - y], yin.at[s], y_send.at[s], y_recv.at[s], to_y, core)
        )
    aux[12:13] = tail
    aux[13:16] = jnp.zeros((3, 128), jnp.float32)
    go(remote(aux, yaux, y_send.at[2], y_recv.at[2], to_y, core))

    def of_spot(spot):
        return (spot // 2) * 4 + y * 2 + spot % 2

    for s in range(seqs):
        pltpu.make_async_copy(yin.at[s], yin.at[s], y_recv.at[s]).wait()
        total_state[s] = (
            state[s, y].astype(jnp.float32) + yin[s].astype(jnp.float32)
        ).astype(jnp.bfloat16)
        for off in range(1, half):
            spot = (spot8 + off) % half
            go(
                remote(
                    total_state.at[s, cut_rows(spot)],
                    rmem.at[spot8, s],
                    m_send.at[s, off],
                    m_recv.at[s, off],
                    of_spot(spot),
                    core,
                )
            )
        rmem[spot8, s] = total_state[s, cut_rows(spot8), :]
    pltpu.make_async_copy(yaux, yaux, y_recv.at[2]).wait()
    keep = (lax.broadcasted_iota(jnp.int32, (16, 128), 0) == 12) & (
        lax.broadcasted_iota(jnp.int32, (16, 128), 1) < seqs
    )
    total_aux[...] = jnp.where(keep, aux[...], aux[...] + yaux[...])
    for off in range(1, half):
        go(
            remote(
                total_aux,
                raux.at[spot8],
                a_send.at[off],
                a_recv.at[off],
                of_spot((spot8 + off) % half),
                core,
            )
        )
    raux[spot8] = total_aux[...]

    def stack(ref):
        return jnp.concatenate([ref[s].astype(jnp.float32) for s in range(seqs)], axis=0)

    queries = stack(new_query)
    own = jnp.sum(queries * stack(new_key), axis=1, keepdims=True) * key_scale
    own_head = (
        lax.broadcasted_iota(jnp.int32, (seqs * heads, heads), 0) % heads
        == lax.broadcasted_iota(jnp.int32, (seqs * heads, heads), 1)
    )

    def upright(block):
        wide = jnp.concatenate(
            [jnp.broadcast_to(block[s : s + 1], (heads, heads)) for s in range(seqs)], axis=0
        )
        return jnp.sum(jnp.where(own_head, wide, 0.0), axis=1, keepdims=True)

    gate_in, gate_f = upright(new_gates[0]), log_sigmoid(upright(new_gates[1]))
    token_values = stack(new_value)

    for off in range(1, half):
        src = (spot8 + half - off) % half
        for s in range(seqs):
            part = rmem.at[src, s]
            pltpu.make_async_copy(part, part, m_recv.at[s, off]).wait()
        pltpu.make_async_copy(raux.at[src], raux.at[src], a_recv.at[off]).wait()

    read_rows, norm_rows, max_rows, dot_rows = [], [], [], []
    for s in range(seqs):
        for h in range(heads):
            srcs = [(a * 2 + h // 2) * 2 + h % 2 for a in range(2)]
            mem = rmem[srcs[0], s].astype(jnp.float32)
            both = raux[srcs[0]]
            for src in srcs[1:]:
                mem = mem + rmem[src, s].astype(jnp.float32)
                both = both + raux[src]
            memory_out[s, h] = mem.astype(jnp.bfloat16)
            read_rows.append(
                jnp.concatenate([both[s * 4 + k : s * 4 + k + 1] for k in range(dv // 128)], 1)
            )
            norm_rows.append(
                jnp.concatenate(
                    [both[8 + s * 2 + k : 9 + s * 2 + k] for k in range(dk // 128)], 1
                )
            )
            max_rows.append(raux[srcs[0], 12:13, s : s + 1])
            dot_rows.append(both[12:13, 2 + s : 3 + s])
    query_state = jnp.concatenate(read_rows, axis=0)
    norm_all = jnp.concatenate(norm_rows, axis=0)
    top = jnp.concatenate(max_rows, axis=0)
    query_norm = jnp.concatenate(dot_rows, axis=0)
    take = (
        lax.broadcasted_iota(jnp.int32, (dk, rows_out), 0)
        == me * rows_out + lax.broadcasted_iota(jnp.int32, (dk, rows_out), 1)
    ).astype(jnp.float32)
    norm_out[...] = jnp.dot(norm_all, take, precision=HIGH, preferred_element_type=jnp.float32)
    max_out[...] = top
    mixed = jnp.maximum(gate_f + top, gate_in)
    carried = jnp.exp(gate_f + top - mixed)
    fresh = jnp.exp(gate_in - mixed)
    numer = carried * query_state + (fresh * own) * token_values
    denom = carried * query_norm + fresh * own
    read_out[...] = (numer / jnp.maximum(jnp.abs(denom), 1.0)).astype(jnp.bfloat16)
    for copy in sent:
        copy.wait_send()


def hand_on(memory, norm, top, read, memory_out, norm_out, max_out, read_out):
    seqs, heads = max_out.shape
    memory_out[...] = memory[...]
    at = lax.broadcasted_iota(jnp.int32, (seqs * heads, heads), 0)
    to = lax.broadcasted_iota(jnp.int32, (seqs * heads, heads), 1)
    wide = read[...].astype(jnp.float32)
    for s in range(seqs):
        rows = slice(s * heads, (s + 1) * heads)
        norm_out[s] = norm[rows]
        read_out[s] = wide[rows].astype(jnp.bfloat16)
        max_out[s : s + 1] = jnp.sum(
            jnp.where(at == s * heads + to, top[...], 0.0), axis=0, keepdims=True
        )


def by_head(
    prompt,
    w_key,
    w_value,
    w_igate,
    w_fgate,
    input_bias,
    forget_bias,
    new_query,
    new_key,
    new_value,
    new_gates,
):
    count = lax.axis_size("sp")
    seqs, span, width = prompt.shape
    depth = w_key.shape[0]
    heads, dk = new_query.shape[1:]
    dv = new_value.shape[2]
    rows = seqs * span
    vmem = pl.BlockSpec(memory_space=pltpu.VMEM)
    hbm = pl.BlockSpec(memory_space=pl.ANY)
    dma = pltpu.SemaphoreType.DMA
    memory, norm, top, read = pl.pallas_call(
        kernel,
        out_shape=(
            jax.ShapeDtypeStruct((seqs, heads, dk // count, dv), jnp.bfloat16),
            jax.ShapeDtypeStruct((seqs * heads, dk // count), jnp.float32),
            jax.ShapeDtypeStruct((seqs * heads, 1), jnp.float32),
            jax.ShapeDtypeStruct((seqs * heads, dv), jnp.bfloat16),
        ),
        in_specs=[hbm, hbm, hbm] + [vmem] * 8,
        out_specs=(vmem, vmem, vmem, vmem),
        scratch_shapes=[
            pltpu.VMEM((4, rows, width), jnp.bfloat16),
            pltpu.VMEM((width, dk), jnp.bfloat16),
            pltpu.VMEM((width, dv), jnp.bfloat16),
            pltpu.VMEM((2 * w_igate.shape[1], width), jnp.bfloat16),
            pltpu.VMEM((4, rows, dk), jnp.float32),
            pltpu.VMEM((4, rows, dv), jnp.float32),
            pltpu.VMEM((4, rows, dk), jnp.bfloat16),
            pltpu.VMEM((4, rows, dv), jnp.bfloat16),
            pltpu.VMEM((4, rows, 128), jnp.float32),
            pltpu.VMEM((4, 8, 128), jnp.float32),
            pltpu.VMEM((seqs, 2, dk // 2, dv), jnp.bfloat16),
            pltpu.VMEM((16, 128), jnp.float32),
            pltpu.VMEM((seqs, dk // 2, dv), jnp.bfloat16),
            pltpu.VMEM((16, 128), jnp.float32),
            pltpu.VMEM((seqs, dk // 2, dv), jnp.bfloat16),
            pltpu.VMEM((16, 128), jnp.float32),
            pltpu.VMEM((count // 2, seqs, dk // count, dv), jnp.bfloat16),
            pltpu.VMEM((count // 2, 16, 128), jnp.float32),
            dma((4,)),
            dma((4, CHUNKS)),
            dma((4, CHUNKS)),
            dma((4, CHUNKS)),
            dma((4, CHUNKS)),
            dma((16,)),
            dma((16,)),
            dma((16,)),
            dma((16,)),
            dma((4,)),
            dma((4,)),
            dma((3,)),
            dma((3,)),
            dma((seqs, count)),
            dma((seqs, count)),
            dma((count,)),
            dma((count,)),
        ],
        compiler_params=pltpu.CompilerParams(
            collective_id=0, has_side_effects=True, vmem_limit_bytes=60 * 1024 * 1024
        ),
    )(
        prompt,
        w_key,
        w_value,
        w_igate.T,
        w_fgate.T,
        input_bias[None],
        forget_bias[None],
        new_query,
        new_key,
        new_value,
        new_gates,
    )
    return pl.pallas_call(
        hand_on,
        out_shape=(
            jax.ShapeDtypeStruct((seqs, heads, dk // count, dv), jnp.bfloat16),
            jax.ShapeDtypeStruct((seqs, heads, dk // count), jnp.float32),
            jax.ShapeDtypeStruct((seqs, heads), jnp.float32),
            jax.ShapeDtypeStruct((seqs, heads, dv), jnp.bfloat16),
        ),
        in_specs=[vmem] * 4,
        out_specs=(vmem,) * 4,
    )(memory, norm, top, read)


def chosen(*args):
    prompt, new_query, new_value = args[0], args[7], args[9]
    heads = new_query.shape[1]
    count = lax.axis_size("sp")
    fits = (
        lax.axis_size("tp") == 2
        and heads == 4
        and count == 16
        and prompt.shape[0] == 2
        and new_query.shape[2] == 256
        and new_value.shape[2] == 512
    )
    return by_head(*args) if fits else per_device(*args)


def entering(value, axis, join, neutral):
    count, mine = (lax.axis_size(axis), lax.axis_index(axis))
    pieces = lax.all_gather(value, axis)
    pieces = pieces[::-1]
    mine = count - 1 - mine
    so_far = jnp.full_like(value, 0) + jnp.asarray(neutral, value.dtype)

    def turn(position, so_far):
        longer = join(so_far, pieces[position])
        return jnp.where(position < mine, longer, so_far)

    return lax.fori_loop(0, count - 1, turn, so_far)


def add_pair(earlier, later):
    return earlier + later


def per_device(
    prompt,
    w_key,
    w_value,
    w_igate,
    w_fgate,
    input_bias,
    forget_bias,
    new_query,
    new_key,
    new_value,
    new_gates,
):
    seq_count, span_len, model_width = prompt.shape
    local_heads = new_query.shape[1]
    key_size = new_query.shape[2]
    value_size = new_value.shape[2]
    key_scale = key_size ** (-0.5)
    token_rows = prompt.reshape(seq_count * span_len, model_width)
    whole_key, whole_value = (
        lax.all_gather(w_key, "sp", axis=0, tiled=True),
        lax.all_gather(w_value, "sp", axis=0, tiled=True),
    )
    key_rows = jnp.dot(token_rows, whole_key, preferred_element_type=jnp.float32).astype(
        jnp.bfloat16
    )
    value_rows = jnp.dot(token_rows, whole_value, preferred_element_type=jnp.float32).astype(
        jnp.bfloat16
    )
    head_start = lax.axis_index("tp") * local_heads
    input_all = jnp.dot(token_rows, w_igate, preferred_element_type=jnp.float32) + input_bias
    forget_all = jnp.dot(token_rows, w_fgate, preferred_element_type=jnp.float32) + forget_bias
    input_gate = lax.dynamic_slice_in_dim(input_all, head_start, local_heads, 1).reshape(
        seq_count, span_len, local_heads
    )
    log_forget = jax.nn.log_sigmoid(
        lax.dynamic_slice_in_dim(forget_all, head_start, local_heads, 1)
    ).reshape(seq_count, span_len, local_heads)
    block_total = jnp.sum(log_forget, axis=1)
    forget_after = block_total[:, None] - jnp.cumsum(log_forget, axis=1)
    log_weight = forget_after + input_gate
    block_max = jnp.max(log_weight, axis=1)
    key_blocks = key_rows.reshape(seq_count, span_len, local_heads, key_size).astype(jnp.float32)
    decayed = (jnp.exp(log_weight - block_max[:, None])[..., None] * key_scale * key_blocks).astype(
        jnp.bfloat16
    )
    value_blocks = value_rows.reshape(seq_count, span_len, local_heads, value_size)
    block_norm = jnp.sum(decayed.astype(jnp.float32), axis=1)
    later_total = entering(block_total, "sp", add_pair, jnp.zeros_like(block_total))
    block_lift = later_total + block_max
    global_max = lax.pmax(block_lift, "sp")
    factor = jnp.exp(block_lift - global_max)
    scaled_norm = factor[:, :, None] * block_norm
    query_full = new_query.astype(jnp.float32)
    block_state = jnp.einsum(
        "sthk,sthv->shkv", decayed, value_blocks, preferred_element_type=jnp.float32
    )
    scaled_state = factor[:, :, None, None] * block_state
    memory_rows, norm_rows = (
        lax.psum_scatter(scaled_state, "sp", scatter_dimension=2, tiled=True),
        lax.psum_scatter(scaled_norm, "sp", scatter_dimension=2, tiled=True),
    )
    token_score = jnp.einsum(
        "shk,sthk->sth", new_query, decayed, preferred_element_type=jnp.float32
    )
    score_high = token_score.astype(jnp.bfloat16)
    score_low = (token_score - score_high.astype(jnp.float32)).astype(jnp.bfloat16)
    weighted = jnp.einsum(
        "sth,sthv->shv", score_high, value_blocks, preferred_element_type=jnp.float32
    )
    weighted = weighted + jnp.einsum(
        "sth,sthv->shv", score_low, value_blocks, preferred_element_type=jnp.float32
    )
    partial_state = factor[..., None] * weighted
    partial_norm = jnp.sum(query_full * scaled_norm, axis=-1)
    query_state, query_norm = lax.psum((partial_state, partial_norm), "sp")
    forget_new = jax.nn.log_sigmoid(new_gates[1])
    input_new = new_gates[0]
    mixed = jnp.maximum(forget_new + global_max, input_new)
    carried = jnp.exp(forget_new + global_max - mixed)
    fresh = jnp.exp(input_new - mixed)
    own_score = jnp.sum(query_full * new_key.astype(jnp.float32), axis=-1) * key_scale
    numer = carried[..., None] * query_state + (fresh * own_score)[..., None] * new_value.astype(
        jnp.float32
    )
    denom = carried * query_norm + fresh * own_score
    first_read = (numer / jnp.maximum(jnp.abs(denom), 1.0)[..., None]).astype(jnp.bfloat16)
    return (memory_rows.astype(jnp.bfloat16), norm_rows, global_max, first_read)


def solution(mesh):
    placed = (
        P(None, "sp", None),
        P("sp", "tp"),
        P("sp", "tp"),
        P(),
        P(),
        P(),
        P(),
        P(None, "tp", None),
        P(None, "tp", None),
        P(None, "tp", None),
        P(None, None, "tp"),
    )
    return jax.shard_map(
        chosen,
        mesh=mesh,
        in_specs=placed,
        out_specs=(
            P(None, "tp", "sp", None),
            P(None, "tp", "sp"),
            P(None, "tp"),
            P(None, "tp", None),
        ),
        check_vma=False,
    )
```

profile of v0, /device:TPU:0, one launch (start us, length us, event | category | flops | bytes accessed | tf_op | source)
XLA Modules:
  0.0 132.6 jit_solution(6391307283061843121)
XLA Ops:
  0.6 130.4 %shard_map.138 = (bf16[2,4,16,512]{3,2,1,0:T(8,128)(2,1)}, f32[8,16]{1,0:T(8,128)}, f32[8,1]{1,0:T(8,128)}, bf16[8,512]{1,0:T(8,128)(2,1)}) custom-call(bf16[2,192,4096]{2,1,0:T(8,128)(2,1)} %prompt.1, bf16[256,1024]{1,0:T(8,128)(2,1)} %w_key.1, bf16[256,2048]{1,0:T(8,128)(2,1)} %w_value.1, bf16[8,4096]{1,0:T(8,128)(2,1)} %bitcast.4, ...), custom_call_target="tpu_custom_call" | custom-call | tf_op jit(solution)/shard_map/pallas_call | solution.py:566
  131.1 1.6 %shard_map.139 = (bf16[2,4,16,512]{3,2,1,0:T(8,128)(2,1)}, f32[2,4,16]{2,1,0:T(4,128)}, f32[2,4]{1,0:T(2,128)}, bf16[2,4,512]{2,1,0:T(4,128)(2,1)}) custom-call(bf16[2,4,16,512]{3,2,1,0:T(8,128)(2,1)} %get-tuple-element.8.memory, f32[8,16]{1,0:T(8,128)} %get-tuple-element.9.norm, f32[8,1]{1,0:T(8,128)} %get-tuple-element.10.top, ...), custom_call_target="tpu_custom_call" | custom-call | tf_op jit(solution)/shard_map/pallas_call | solution.py:629
where the time goes:
time: 133 us
  Pallas kernels  132 us (99%)
    pallas_call x1, Pallas kernels, by_head(): pl.pallas_call(kernel, out_shape=(jax.ShapeDtypeStruct((seqs, heads, dk /...  130 us

commit v1 on v0

v1 whole, which is shorter than its diff:
```python
import functools
import jax
import jax.numpy as jnp
from jax import lax
from jax.experimental import pallas as pl
from jax.experimental.pallas import tpu as pltpu
from jax.sharding import PartitionSpec as P

HIGH = lax.Precision.HIGHEST
UNITS = 8
SENDS = 160


def flip(bit, change):
    return bit + change - 2 * bit * change


def log_sigmoid(v):
    return jnp.minimum(v, 0.0) - jnp.log1p(jnp.exp(-jnp.abs(v)))


def iota(shape, dim):
    return lax.broadcasted_iota(jnp.int32, shape, dim)


def kernel(
    prompt,
    w_key,
    w_value,
    w_igate,
    w_fgate,
    input_bias,
    forget_bias,
    new_query,
    new_key,
    new_value,
    new_gates,
    memory_out,
    norm_out,
    max_out,
    read_out,
    xb,
    wb,
    pass_w,
    acc,
    decay,
    vals,
    weight,
    gate_w,
    stat,
    state,
    aux,
    rmem,
    raux,
    local_sem,
    sends,
    x_recv,
    d_recv,
    w_recv,
    g_recv,
    s_recv,
    m_recv,
    a_recv,
):
    count = lax.axis_size("sp")
    me = lax.axis_index("sp")
    core = lax.axis_index("tp")
    seqs, span, width = prompt.shape
    depth = w_key.shape[0]
    heads = new_query.shape[1]
    dk = new_query.shape[2]
    dv = new_value.shape[2]
    total_heads = input_bias.shape[1]
    key_scale = dk ** (-0.5)
    per_seq = UNITS // seqs
    cut = width // (2 * per_seq)
    rows_out = dk // count
    zh, zl, y, x = me // 8, (me // 4) % 2, (me // 2) % 2, me % 2
    mine = zl * 2 + x
    inner = zh != zl
    bf16, f32 = jnp.bfloat16, jnp.float32

    def place(dh, dl, dy, dx):
        return flip(zh, dh) * 8 + flip(zl, dl) * 4 + flip(y, dy) * 2 + flip(x, dx)

    sent = []

    def remote(src, dst, recv, sp, tp, when=None):
        copy = pltpu.make_async_remote_copy(
            src_ref=src,
            dst_ref=dst,
            send_sem=sends.at[len(sent)],
            recv_sem=recv,
            device_id=(sp, tp),
            device_id_type=pl.DeviceIdType.MESH,
        )
        sent.append((copy, when))
        return copy

    def start(copies, when=None):
        def run():
            for copy in copies:
                copy.start()

        if when is None:
            run()
        else:
            pl.when(when)(run)

    def landed(ref, sem):
        pltpu.make_async_copy(ref, ref, sem).wait()

    barrier = pltpu.get_barrier_semaphore()
    for off in range(1, count):
        pl.semaphore_signal(
            barrier,
            inc=1,
            device_id=((me + off) % count, core),
            device_id_type=pl.DeviceIdType.MESH,
        )
    pl.semaphore_signal(
        barrier, inc=1, device_id=(me, 1 - core), device_id_type=pl.DeviceIdType.MESH
    )

    def bits(slot):
        return slot // 8, (slot // 4) % 2, (slot // 2) % 2, slot % 2

    def w_rows(slot):
        return pl.ds(pl.multiple_of(place(*bits(slot)) * depth, depth), depth)

    def group_cols(dl, dx):
        group = flip(zl, dl) * 2 + flip(x, dx)
        kc = pl.ds(pl.multiple_of(group * dk, dk), dk)
        vc = pl.ds(pl.multiple_of(group * dv, dv), dv)
        return kc, vc

    own_x = []
    for s in range(seqs):
        c = pltpu.make_async_copy(
            prompt.at[s], xb.at[0, pl.ds(s * span, span)], local_sem.at[s]
        )
        c.start()
        own_x.append(c)
    kc, vc = group_cols(0, 0)
    own_w = [
        pltpu.make_async_copy(w_key.at[:, kc], wb.at[w_rows(0), :dk], local_sem.at[2]),
        pltpu.make_async_copy(w_value.at[:, vc], wb.at[w_rows(0), dk:], local_sem.at[3]),
    ]
    for c in own_w:
        c.start()
    pl.semaphore_wait(barrier, count)

    to_x, to_y, to_z = place(0, 0, 0, 1), place(0, 0, 1, 0), place(0, 1, 0, 0)
    to_far, to_mid = place(1, 0, 0, 0), place(1, 1, 0, 0)

    def w_own(dl, dx, peer, slot, when=None):
        kc, vc = group_cols(dl, dx)
        rows = w_rows(0)
        return [
            remote(w_key.at[:, kc], wb.at[rows, :dk], w_recv.at[slot], peer, core, when),
            remote(w_value.at[:, vc], wb.at[rows, dk:], w_recv.at[slot], peer, core, when),
        ]

    def w_relay(slot, peer, there, when=None):
        rows = w_rows(slot)
        return [remote(wb.at[rows], wb.at[rows], w_recv.at[there], peer, core, when)]

    def w_wait(slot):
        landed(wb.at[w_rows(slot)], w_recv.at[slot])

    def part(block, unit, owner):
        s, k = unit // per_seq, unit % per_seq
        cols = pl.ds(pl.multiple_of((owner * per_seq + k) * cut, cut), cut)
        return xb.at[block, pl.ds(s * span, span), cols]

    def x_own(block, unit, peer):
        s, k = unit // per_seq, unit % per_seq
        cols = pl.ds(pl.multiple_of((core * per_seq + k) * cut, cut), cut)
        return [
            remote(
                prompt.at[s, :, cols],
                part(block, unit, core),
                x_recv.at[block, unit],
                peer,
                core,
            )
        ]

    def x_relay(unit):
        return [
            remote(part(2, unit, core), part(3, unit, core), x_recv.at[3, unit], to_x, core)
        ]

    def x_across(block, unit):
        own = part(block, unit, core)
        return [remote(own, own, d_recv.at[block, unit], me, 1 - core)]

    def x_wait(block, unit):
        landed(part(block, unit, core), x_recv.at[block, unit])

    def d_wait(block, unit):
        landed(part(block, unit, 1 - core), d_recv.at[block, unit])

    def go_x(block, units):
        for unit in units:
            x_wait(block, unit)
            if block == 2:
                start(x_relay(unit))
            start(x_across(block, unit))

    def d_all(block, s):
        for unit in range(s * per_seq, (s + 1) * per_seq):
            d_wait(block, unit)

    def go_w(slot):
        w_wait(slot)
        start(w_relay(slot, to_y, slot + 2))

    first = core == 0

    near, far, mid = (
        w_own(1, 0, to_z, 4),
        w_own(0, 0, to_far, 8),
        w_own(1, 0, to_mid, 12, inner),
    )
    tokens = [x_own(2, unit, to_z) for unit in range(UNITS)]
    px = w_own(0, 1, to_x, 1)
    kc, vc = group_cols(1, 1)
    px2 = [
        remote(w_key.at[:, kc], pass_w.at[:, :dk], w_recv.at[0], to_x, core),
        remote(w_value.at[:, vc], pass_w.at[:, dk:], w_recv.at[0], to_x, core),
    ]
    start(px)
    start(w_own(0, 0, to_y, 2))

    @pl.when(first)
    def _():
        start(far)
        start(near)

    @pl.when(core == 1)
    def _():
        start(near)
        start(far)

    start(px2)
    start(mid, inner)
    for unit in range(2):
        start(tokens[unit])
    for unit in range(UNITS):
        start(x_own(1, unit, to_x))

    w_gate = jnp.concatenate([w_igate[...], w_fgate[...]], axis=0)
    square = iota((total_heads, total_heads), 0) == iota((total_heads, total_heads), 1)

    def upright(row):
        return jnp.sum(jnp.where(square, row, 0.0), axis=1, keepdims=True)

    bias_in, bias_f = upright(input_bias[...]), upright(forget_bias[...])
    after = (iota((span, span), 0) > iota((span, span), 1)).astype(f32)
    spot_head = iota((total_heads, 128), 0) - core * heads
    spot_lane = iota((total_heads, 128), 1)
    local_head = (spot_head >= 0) & (spot_head < heads)
    for c in own_x:
        c.wait()
    packed = jnp.zeros((1, 128), f32)
    gate_w[0] = jnp.zeros(gate_w.shape[1:], f32)
    for s in range(seqs):
        both = lax.dot_general(
            w_gate,
            xb[0, s * span : (s + 1) * span],
            (((1,), (1,)), ((), ())),
            preferred_element_type=f32,
        )
        gate_in = both[:total_heads] + bias_in
        forget = log_sigmoid(both[total_heads:] + bias_f)
        level = gate_in + jnp.dot(forget, after, precision=HIGH, preferred_element_type=f32)
        top = jnp.max(level, axis=1, keepdims=True)
        total = jnp.sum(forget, axis=1, keepdims=True)
        part_w = jnp.exp(level - top) * key_scale
        gate_w[0, s * heads : (s + 1) * heads, :span] = jnp.where(
            first, part_w[:heads], part_w[heads : 2 * heads]
        )
        at = spot_lane - s * heads
        packed = packed + jnp.sum(
            jnp.where(local_head & (at == spot_head), total, 0.0)
            + jnp.where(local_head & (at - seqs * heads == spot_head), top, 0.0),
            axis=0,
            keepdims=True,
        )
    stat[me] = jnp.broadcast_to(packed, (8, 128))
    for block in (1, 2, 3):
        start(
            [
                remote(
                    gate_w.at[0],
                    gate_w.at[block],
                    g_recv.at[block],
                    place(0, block // 2, 0, block % 2),
                    core,
                )
            ]
        )
    for off in range(count - 1, 0, -1):
        peer = place(*bits(off))
        start([remote(stat.at[me], stat.at[me], s_recv, peer, core)])
    for c in own_w:
        c.wait()

    def multiply(blocks, slots, s=None):
        low, size = (0, seqs * span) if s is None else (s * span, span)
        pairs = len(slots) // 2

        def choose(i, values):
            out = jnp.int32(values[0])
            for k, v in enumerate(values[1:], 1):
                out = jnp.where(i == k, v, out)
            return out

        def step(i, carry):
            block = choose(i // pairs, blocks) if len(blocks) > 1 else blocks[0]
            at = i % pairs
            out = None
            for off in range(2):
                slot = choose(at, slots[off::2]) if pairs > 1 else slots[off]
                rows = w_rows(slot)
                piece = jnp.dot(
                    xb[block, pl.ds(low, size), rows], wb[rows], preferred_element_type=f32
                )
                out = piece if out is None else out + piece
            acc[block, pl.ds(low, size)] += out
            return carry

        lax.fori_loop(0, len(blocks) * pairs, step, 0)

    for block in range(4):
        acc[block] = jnp.zeros(acc.shape[1:], f32)

    eye = (iota((span, span), 0) == iota((span, span), 1)).astype(f32)
    here = iota((span, seqs * heads), 1)
    chip = iota((count, seqs * heads), 0)
    lane16 = iota((count, seqs * heads), 1)

    def weigh():
        landed(stat.at[pl.ds(0, count - 1)], s_recv)
        table = jnp.concatenate([stat[c, 0:1] for c in range(count)], axis=0)
        beyond = (iota((count, count), 1) > iota((count, count), 0)).astype(f32)
        later = jnp.dot(beyond, table, precision=HIGH, preferred_element_type=f32)
        lift = later[:, : seqs * heads] + table[:, seqs * heads : 2 * seqs * heads]
        highest = jnp.max(lift, axis=0, keepdims=True)
        factor = jnp.exp(lift - highest)
        for block in range(4):
            if block:
                landed(gate_w.at[block], g_recv.at[block])
            turned = lax.dot_general(
                eye,
                gate_w[block][:, :span],
                (((1,), (1,)), ((), ())),
                precision=HIGH,
                preferred_element_type=f32,
            )
            for s in range(seqs):
                column = jnp.sum(
                    jnp.where(here == s * heads + mine, turned, 0.0), axis=1, keepdims=True
                )
                hit = (chip == place(0, block // 2, 0, block % 2)) & (lane16 == s * heads + mine)
                scale = jnp.sum(jnp.where(hit, factor, 0.0), keepdims=True)
                weight[block, s * span : (s + 1) * span] = jnp.broadcast_to(
                    column * scale, (span, 128)
                )
        return highest

    def finish(block, s):
        rows = slice(s * span, (s + 1) * span)
        to = slice(block * span, (block + 1) * span)
        keys = acc[block, rows, :dk].astype(bf16).astype(f32)
        decay[s, to] = (weight[block, rows, 0:1] * keys).astype(bf16)
        vals[s, to] = acc[block, rows, dk:].astype(bf16)

    ones = jnp.ones((8, 4 * span), bf16)
    pick = iota((heads, dk), 0) == mine

    def out_rows(chip):
        return pl.ds(pl.multiple_of(chip * rows_out, rows_out), rows_out)

    def reduce(s):
        d = decay[s]
        sums = lax.dot_general(
            d, vals[s], (((0,), (0,)), ((), ())), preferred_element_type=f32
        )
        high = sums.astype(bf16)
        state[s] = high
        for off in range(count - 1, 0, -1):
            peer = place(*bits(off))
            start(
                [remote(state.at[s, out_rows(peer)], rmem.at[s, me], m_recv.at[s], peer, core)]
            )
        low = (sums - high.astype(f32)).astype(bf16)
        norms = jnp.dot(ones, d, preferred_element_type=f32)
        query = jnp.sum(
            jnp.where(pick, new_query[s].astype(f32), 0.0), axis=0, keepdims=True
        )
        wide = jnp.broadcast_to(query, (8, dk)).astype(bf16)
        seen = jnp.dot(wide, high, preferred_element_type=f32) + jnp.dot(
            wide, low, preferred_element_type=f32
        )
        for k in range(dv // 128):
            aux[s, k : k + 1] = seen[0:1, k * 128 : (k + 1) * 128]
        for k in range(dk // 128):
            aux[s, 4 + k : 5 + k] = norms[0:1, k * 128 : (k + 1) * 128]
        dot_norm = jnp.sum(query * norms[0:1], axis=1, keepdims=True)
        aux[s, 6:8] = jnp.broadcast_to(dot_norm, (2, 128))
        for off in range(count - 1, 0, -1):
            start([remote(aux.at[s], raux.at[s, me], a_recv.at[s], place(*bits(off)), core)])
        rmem[s, me] = state[s, out_rows(me)]
        raux[s, me] = aux[s]

    w_wait(1)
    start(w_relay(1, to_far, 9))
    start(w_relay(1, to_y, 3))
    w_wait(4)
    start(w_relay(4, to_y, 6))
    start(w_relay(4, to_far, 12, inner), inner)
    w_wait(2)
    multiply([0], [0, 2, 1, 4])
    landed(pass_w, w_recv.at[0])
    start([remote(pass_w, wb.at[w_rows(1)], w_recv.at[5], to_z, core)])
    start(tokens[2])
    start([remote(pass_w, wb.at[w_rows(1)], w_recv.at[13], to_mid, core, inner)], inner)
    for unit in range(3, UNITS):
        start(tokens[unit])
    go_w(8)
    w_wait(3)
    multiply([0], [8, 3])
    go_x(1, (0, 1))
    highest = weigh()
    go_w(5)
    start(w_relay(5, to_far, 13, inner), inner)
    w_wait(6)
    go_x(1, (2, 3))
    multiply([0], [5, 6])
    go_w(12)
    w_wait(10)
    go_x(2, (0, 1))
    multiply([0], [12, 10])
    go_x(1, (4, 5))
    go_x(2, (2, 3))
    d_all(1, 0)
    multiply([1], [0, 2, 1, 4, 8, 3, 5, 6, 12, 10], 0)
    go_x(1, (6, 7))
    go_w(9)
    w_wait(7)
    multiply([0], [9, 7])
    go_x(2, (4,))
    d_all(1, 1)
    multiply([1], [0, 2, 1, 4, 8, 3, 5, 6, 12, 10], 1)
    d_all(2, 0)
    go_x(2, (5,))
    multiply([2], [0, 2, 1, 4, 8, 3, 5, 6, 12, 10], 0)
    go_x(3, (0, 1))
    go_x(2, (6,))
    go_w(13)
    w_wait(14)
    go_x(3, (2, 3))
    multiply([0, 1], [13, 14])
    multiply([1], [9, 7])
    go_x(2, (7,))
    d_all(3, 0)
    multiply([3], [0, 2, 1, 4, 8, 3, 5, 6, 12, 10], 0)
    multiply([2, 3], [9, 7, 13, 14], 0)
    go_x(3, (4, 5))
    d_all(2, 1)
    multiply([2], [0, 2, 1, 4, 8, 3, 5, 6, 12, 10, 9, 7, 13, 14], 1)
    w_wait(11)
    w_wait(15)
    go_x(3, (6,))
    multiply([0, 1, 2, 3], [11, 15], 0)
    for block in range(4):
        finish(block, 0)
    reduce(0)
    go_x(3, (7,))
    multiply([0, 1, 2], [11, 15], 1)
    for block in range(3):
        finish(block, 1)
    d_all(3, 1)
    multiply([3], [0, 2, 1, 4, 8, 3, 5, 6, 12, 10, 9, 7, 13, 14, 11, 15], 1)
    finish(3, 1)
    reduce(1)

    def stack(ref):
        return jnp.concatenate([ref[s].astype(f32) for s in range(seqs)], axis=0)

    queries = stack(new_query)
    own = jnp.sum(queries * stack(new_key), axis=1, keepdims=True) * key_scale
    own_head = iota((seqs * heads, heads), 0) % heads == iota((seqs * heads, heads), 1)

    def gate_column(block):
        wide = jnp.concatenate(
            [jnp.broadcast_to(block[s : s + 1], (heads, heads)) for s in range(seqs)], axis=0
        )
        return jnp.sum(jnp.where(own_head, wide, 0.0), axis=1, keepdims=True)

    gate_in, gate_f = gate_column(new_gates[0]), log_sigmoid(gate_column(new_gates[1]))
    token_values = stack(new_value)
    top = upright(highest)
    max_out[...] = top

    read_rows, norm_rows, dot_rows = [], [], []
    for s in range(seqs):
        landed(rmem.at[s, pl.ds(0, count - 1)], m_recv.at[s])
        landed(raux.at[s, pl.ds(0, count - 1)], a_recv.at[s])
        for h in range(heads):
            srcs = [
                (a * 2 + h // 2) * 4 + b * 2 + h % 2 for a in range(2) for b in range(2)
            ]
            mem = rmem[s, srcs[0]].astype(f32)
            both = raux[s, srcs[0]]
            for src in srcs[1:]:
                mem = mem + rmem[s, src].astype(f32)
                both = both + raux[s, src]
            memory_out[s, h] = mem.astype(bf16)
            read_rows.append(
                jnp.concatenate([both[k : k + 1] for k in range(dv // 128)], 1)
            )
            norm_rows.append(
                jnp.concatenate([both[4 + k : 5 + k] for k in range(dk // 128)], 1)
            )
            dot_rows.append(both[6:7, 0:1])
    query_state = jnp.concatenate(read_rows, axis=0)
    norm_all = jnp.concatenate(norm_rows, axis=0)
    query_norm = jnp.concatenate(dot_rows, axis=0)
    take = (
        iota((dk, rows_out), 0) == me * rows_out + iota((dk, rows_out), 1)
    ).astype(f32)
    norm_out[...] = jnp.dot(norm_all, take, precision=HIGH, preferred_element_type=f32)
    mixed = jnp.maximum(gate_f + top, gate_in)
    carried = jnp.exp(gate_f + top - mixed)
    fresh = jnp.exp(gate_in - mixed)
    numer = carried * query_state + (fresh * own) * token_values
    denom = carried * query_norm + fresh * own
    read_out[...] = (numer / jnp.maximum(jnp.abs(denom), 1.0)).astype(bf16)
    for copy, when in sent:
        if when is None:
            copy.wait_send()
        else:
            pl.when(when)(copy.wait_send)


def hand_on(memory, norm, top, read, memory_out, norm_out, max_out, read_out):
    seqs, heads = max_out.shape
    memory_out[...] = memory[...]
    at = lax.broadcasted_iota(jnp.int32, (seqs * heads, heads), 0)
    to = lax.broadcasted_iota(jnp.int32, (seqs * heads, heads), 1)
    wide = read[...].astype(jnp.float32)
    for s in range(seqs):
        rows = slice(s * heads, (s + 1) * heads)
        norm_out[s] = norm[rows]
        read_out[s] = wide[rows].astype(jnp.bfloat16)
        max_out[s : s + 1] = jnp.sum(
            jnp.where(at == s * heads + to, top[...], 0.0), axis=0, keepdims=True
        )


def by_head(
    prompt,
    w_key,
    w_value,
    w_igate,
    w_fgate,
    input_bias,
    forget_bias,
    new_query,
    new_key,
    new_value,
    new_gates,
):
    count = lax.axis_size("sp")
    seqs, span, width = prompt.shape
    depth = w_key.shape[0]
    heads, dk = new_query.shape[1:]
    dv = new_value.shape[2]
    rows = seqs * span
    vmem = pl.BlockSpec(memory_space=pltpu.VMEM)
    hbm = pl.BlockSpec(memory_space=pl.ANY)
    dma = pltpu.SemaphoreType.DMA
    memory, norm, top, read = pl.pallas_call(
        kernel,
        out_shape=(
            jax.ShapeDtypeStruct((seqs, heads, dk // count, dv), jnp.bfloat16),
            jax.ShapeDtypeStruct((seqs * heads, dk // count), jnp.float32),
            jax.ShapeDtypeStruct((seqs * heads, 1), jnp.float32),
            jax.ShapeDtypeStruct((seqs * heads, dv), jnp.bfloat16),
        ),
        in_specs=[hbm, hbm, hbm] + [vmem] * 8,
        out_specs=(vmem, vmem, vmem, vmem),
        scratch_shapes=[
            pltpu.VMEM((4, rows, width), jnp.bfloat16),
            pltpu.VMEM((width, dk + dv), jnp.bfloat16),
            pltpu.VMEM((depth, dk + dv), jnp.bfloat16),
            pltpu.VMEM((4, rows, dk + dv), jnp.float32),
            pltpu.VMEM((seqs, 4 * span, dk), jnp.bfloat16),
            pltpu.VMEM((seqs, 4 * span, dv), jnp.bfloat16),
            pltpu.VMEM((4, rows, 128), jnp.float32),
            pltpu.VMEM((4, 8, 256), jnp.float32),
            pltpu.VMEM((count, 8, 128), jnp.float32),
            pltpu.VMEM((seqs, dk, dv), jnp.bfloat16),
            pltpu.VMEM((seqs, 8, 128), jnp.float32),
            pltpu.VMEM((seqs, count, dk // count, dv), jnp.bfloat16),
            pltpu.VMEM((seqs, count, 8, 128), jnp.float32),
            dma((4,)),
            dma((SENDS,)),
            dma((4, UNITS)),
            dma((4, UNITS)),
            dma((16,)),
            dma((4,)),
            dma,
            dma((seqs,)),
            dma((seqs,)),
        ],
        compiler_params=pltpu.CompilerParams(
            collective_id=0, has_side_effects=True, vmem_limit_bytes=60 * 1024 * 1024
        ),
    )(
        prompt,
        w_key,
        w_value,
        w_igate.T,
        w_fgate.T,
        input_bias[None],
        forget_bias[None],
        new_query,
        new_key,
        new_value,
        new_gates,
    )
    return pl.pallas_call(
        hand_on,
        out_shape=(
            jax.ShapeDtypeStruct((seqs, heads, dk // count, dv), jnp.bfloat16),
            jax.ShapeDtypeStruct((seqs, heads, dk // count), jnp.float32),
            jax.ShapeDtypeStruct((seqs, heads), jnp.float32),
            jax.ShapeDtypeStruct((seqs, heads, dv), jnp.bfloat16),
        ),
        in_specs=[vmem] * 4,
        out_specs=(vmem,) * 4,
    )(memory, norm, top, read)


def chosen(*args):
    prompt, new_query, new_value = args[0], args[7], args[9]
    heads = new_query.shape[1]
    count = lax.axis_size("sp")
    fits = (
        lax.axis_size("tp") == 2
        and heads == 4
        and count == 16
        and prompt.shape[0] == 2
        and new_query.shape[2] == 256
        and new_value.shape[2] == 512
    )
    return by_head(*args) if fits else per_device(*args)


def entering(value, axis, join, neutral):
    count, mine = (lax.axis_size(axis), lax.axis_index(axis))
    pieces = lax.all_gather(value, axis)
    pieces = pieces[::-1]
    mine = count - 1 - mine
    so_far = jnp.full_like(value, 0) + jnp.asarray(neutral, value.dtype)

    def turn(position, so_far):
        longer = join(so_far, pieces[position])
        return jnp.where(position < mine, longer, so_far)

    return lax.fori_loop(0, count - 1, turn, so_far)


def add_pair(earlier, later):
    return earlier + later


def per_device(
    prompt,
    w_key,
    w_value,
    w_igate,
    w_fgate,
    input_bias,
    forget_bias,
    new_query,
    new_key,
    new_value,
    new_gates,
):
    seq_count, span_len, model_width = prompt.shape
    local_heads = new_query.shape[1]
    key_size = new_query.shape[2]
    value_size = new_value.shape[2]
    key_scale = key_size ** (-0.5)
    token_rows = prompt.reshape(seq_count * span_len, model_width)
    whole_key, whole_value = (
        lax.all_gather(w_key, "sp", axis=0, tiled=True),
        lax.all_gather(w_value, "sp", axis=0, tiled=True),
    )
    key_rows = jnp.dot(token_rows, whole_key, preferred_element_type=jnp.float32).astype(
        jnp.bfloat16
    )
    value_rows = jnp.dot(token_rows, whole_value, preferred_element_type=jnp.float32).astype(
        jnp.bfloat16
    )
    head_start = lax.axis_index("tp") * local_heads
    input_all = jnp.dot(token_rows, w_igate, preferred_element_type=jnp.float32) + input_bias
    forget_all = jnp.dot(token_rows, w_fgate, preferred_element_type=jnp.float32) + forget_bias
    input_gate = lax.dynamic_slice_in_dim(input_all, head_start, local_heads, 1).reshape(
        seq_count, span_len, local_heads
    )
    log_forget = jax.nn.log_sigmoid(
        lax.dynamic_slice_in_dim(forget_all, head_start, local_heads, 1)
    ).reshape(seq_count, span_len, local_heads)
    block_total = jnp.sum(log_forget, axis=1)
    forget_after = block_total[:, None] - jnp.cumsum(log_forget, axis=1)
    log_weight = forget_after + input_gate
    block_max = jnp.max(log_weight, axis=1)
    key_blocks = key_rows.reshape(seq_count, span_len, local_heads, key_size).astype(jnp.float32)
    decayed = (jnp.exp(log_weight - block_max[:, None])[..., None] * key_scale * key_blocks).astype(
        jnp.bfloat16
    )
    value_blocks = value_rows.reshape(seq_count, span_len, local_heads, value_size)
    block_norm = jnp.sum(decayed.astype(jnp.float32), axis=1)
    later_total = entering(block_total, "sp", add_pair, jnp.zeros_like(block_total))
    block_lift = later_total + block_max
    global_max = lax.pmax(block_lift, "sp")
    factor = jnp.exp(block_lift - global_max)
    scaled_norm = factor[:, :, None] * block_norm
    query_full = new_query.astype(jnp.float32)
    block_state = jnp.einsum(
        "sthk,sthv->shkv", decayed, value_blocks, preferred_element_type=jnp.float32
    )
    scaled_state = factor[:, :, None, None] * block_state
    memory_rows, norm_rows = (
        lax.psum_scatter(scaled_state, "sp", scatter_dimension=2, tiled=True),
        lax.psum_scatter(scaled_norm, "sp", scatter_dimension=2, tiled=True),
    )
    token_score = jnp.einsum(
        "shk,sthk->sth", new_query, decayed, preferred_element_type=jnp.float32
    )
    score_high = token_score.astype(jnp.bfloat16)
    score_low = (token_score - score_high.astype(jnp.float32)).astype(jnp.bfloat16)
    weighted = jnp.einsum(
        "sth,sthv->shv", score_high, value_blocks, preferred_element_type=jnp.float32
    )
    weighted = weighted + jnp.einsum(
        "sth,sthv->shv", score_low, value_blocks, preferred_element_type=jnp.float32
    )
    partial_state = factor[..., None] * weighted
    partial_norm = jnp.sum(query_full * scaled_norm, axis=-1)
    query_state, query_norm = lax.psum((partial_state, partial_norm), "sp")
    forget_new = jax.nn.log_sigmoid(new_gates[1])
    input_new = new_gates[0]
    mixed = jnp.maximum(forget_new + global_max, input_new)
    carried = jnp.exp(forget_new + global_max - mixed)
    fresh = jnp.exp(input_new - mixed)
    own_score = jnp.sum(query_full * new_key.astype(jnp.float32), axis=-1) * key_scale
    numer = carried[..., None] * query_state + (fresh * own_score)[..., None] * new_value.astype(
        jnp.float32
    )
    denom = carried * query_norm + fresh * own_score
    first_read = (numer / jnp.maximum(jnp.abs(denom), 1.0)[..., None]).astype(jnp.bfloat16)
    return (memory_rows.astype(jnp.bfloat16), norm_rows, global_max, first_read)


def solution(mesh):
    placed = (
        P(None, "sp", None),
        P("sp", "tp"),
        P("sp", "tp"),
        P(),
        P(),
        P(),
        P(),
        P(None, "tp", None),
        P(None, "tp", None),
        P(None, "tp", None),
        P(None, None, "tp"),
    )
    return jax.shard_map(
        chosen,
        mesh=mesh,
        in_specs=placed,
        out_specs=(
            P(None, "tp", "sp", None),
            P(None, "tp", "sp"),
            P(None, "tp"),
            P(None, "tp", None),
        ),
        check_vma=False,
    )
```

time: 133 us -> 121 us (0.910)
  Pallas kernels: 132 us -> 120 us
    pallas_call x1, Pallas kernels: 130 us -> 118 us  [by_head(): pl.pallas_call(kernel, out_shape=(jax.ShapeDtypeStruct((seqs, heads, dk /...]
where the time goes in v1:
time: 121 us; the launch traced here: 120 us
  Pallas kernels  120 us (99%)
    pallas_call x1, Pallas kernels, by_head(): pl.pallas_call(kernel, out_shape=(jax.ShapeDtypeStruct((seqs, heads, dk /...  118 us

profile of v1, /device:TPU:0, one launch (start us, length us, event | category | flops | bytes accessed | tf_op | source)
XLA Modules:
  0.0 120.5 jit_solution(18258988941616684547)
XLA Ops:
  0.6 118.2 %shard_map.138 = (bf16[2,4,16,512]{3,2,1,0:T(8,128)(2,1)}, f32[8,16]{1,0:T(8,128)}, f32[8,1]{1,0:T(8,128)}, bf16[8,512]{1,0:T(8,128)(2,1)}) custom-call(bf16[2,192,4096]{2,1,0:T(8,128)(2,1)} %prompt.1, bf16[256,1024]{1,0:T(8,128)(2,1)} %w_key.1, bf16[256,2048]{1,0:T(8,128)(2,1)} %w_value.1, bf16[8,4096]{1,0:T(8,128)(2,1)} %bitcast.4, ...), custom_call_target="tpu_custom_call" | custom-call | tf_op jit(solution)/shard_map/pallas_call | solution.py:586
  118.9 1.6 %shard_map.139 = (bf16[2,4,16,512]{3,2,1,0:T(8,128)(2,1)}, f32[2,4,16]{2,1,0:T(4,128)}, f32[2,4]{1,0:T(2,128)}, bf16[2,4,512]{2,1,0:T(4,128)(2,1)}) custom-call(bf16[2,4,16,512]{3,2,1,0:T(8,128)(2,1)} %get-tuple-element.8.memory, f32[8,16]{1,0:T(8,128)} %get-tuple-element.9.norm, f32[8,1]{1,0:T(8,128)} %get-tuple-element.10.top, ...), custom_call_target="tpu_custom_call" | custom-call | tf_op jit(solution)/shard_map/pallas_call | solution.py:636

commit v2 on v1

--- a/solution.py
+++ b/solution.py
@@ -7,8 +7,151 @@
 from jax.sharding import PartitionSpec as P
 
 HIGH = lax.Precision.HIGHEST
-UNITS = 8
-SENDS = 160
+PARTS = 4
+KINDS = ("x1", "x2", "x3", "xa", "ya", "xb", "yb", "xc", "yc")
+SENDS = 180
+SCHEDULE = (
+    ("far",),
+    ("px2",),
+    ("tx", 0),
+    ("mid",),
+    ("tz", 0),
+    ("near",),
+    ("px",),
+    ("tx", 1),
+    ("yown",),
+    ("x2", 0),
+    ("tx", 2),
+    ("w", 8),
+    ("tb", 0),
+    ("tx", 3),
+    ("tz", 1),
+    ("p",),
+    ("w", 4),
+    ("w", 1),
+    ("tz", 2),
+    ("pm",),
+    ("tx", 4),
+    ("w", 12),
+    ("tx", 5),
+    ("x1", 0),
+    ("x1", 1),
+    ("x2", 1),
+    ("tx", 6),
+    ("tz", 3),
+    ("w", 2),
+    ("w", 5),
+    ("x1", 2),
+    ("xb", 0),
+    ("x3", 0),
+    ("x1", 3),
+    ("gates",),
+    ("w", 3),
+    ("x1", 4),
+    ("x1", 5),
+    ("ta", 0),
+    ("tb", 1),
+    ("ta", 1),
+    ("tx", 7),
+    ("x1", 6),
+    ("mm", 0, 2, (8, 4, 1, 12)),
+    ("x2", 2),
+    ("w", 10),
+    ("x3", 1),
+    ("mm", 0, 2, (2, 5, 0, 3)),
+    ("ta", 2),
+    ("yb", 0),
+    ("w", 9),
+    ("x1", 7),
+    ("x2", 3),
+    ("d", "x1", 0),
+    ("d", "x1", 4),
+    ("mm", 2, 2, (8, 4, 1, 12)),
+    ("yb", 1),
+    ("w", 6),
+    ("mm", 2, 2, (2, 5, 0, 3)),
+    ("xc", 0),
+    ("w", 14),
+    ("tell_all",),
+    ("x3", 2),
+    ("ta", 3),
+    ("w", 13),
+    ("tb", 2),
+    ("xa", 0),
+    ("xa", 1),
+    ("x3", 3),
+    ("tb", 3),
+    ("d", "x2", 0),
+    ("d", "x3", 0),
+    ("mm", 4, 2, (8, 4, 1, 12)),
+    ("mm", 2, 2, (10, 9, 6, 14)),
+    ("mm", 4, 2, (2, 5, 0, 3)),
+    ("xa", 2),
+    ("mm", 0, 2, (10, 9, 6, 14)),
+    ("yb", 2),
+    ("yc", 0),
+    ("yb", 3),
+    ("mm", 4, 2, (10, 9, 6, 14)),
+    ("xc", 1),
+    ("w", 7),
+    ("xc", 2),
+    ("ya", 0),
+    ("xa", 3),
+    ("weigh",),
+    ("xc", 3),
+    ("ya", 1),
+    ("w", 11),
+    ("xb", 1),
+    ("w", 15),
+    ("mm", 4, 2, (13, 7, 11, 15)),
+    ("mm", 0, 2, (13, 7, 11, 15)),
+    ("mm", 2, 2, (13, 7, 11, 15)),
+    ("finish", 0, 2, 4, 5),
+    ("reduce", 0),
+    ("d1", "xa", 0),
+    ("d1", "ya", 0),
+    ("mma", 6, 1, 0),
+    ("d1", "xb", 0),
+    ("d1", "yb", 0),
+    ("d1", "xc", 0),
+    ("d1", "yc", 0),
+    ("mma", 7, 2, 0),
+    ("yc", 1),
+    ("d1", "xa", 1),
+    ("d1", "ya", 1),
+    ("mma", 6, 1, 1),
+    ("d1", "xb", 1),
+    ("d1", "yb", 1),
+    ("d1", "xc", 1),
+    ("d1", "yc", 1),
+    ("mma", 7, 2, 1),
+    ("ya", 2),
+    ("yc", 2),
+    ("xb", 2),
+    ("ya", 3),
+    ("xb", 3),
+    ("yc", 3),
+    ("d1", "xa", 2),
+    ("d1", "ya", 2),
+    ("mma", 6, 1, 2),
+    ("d1", "xb", 2),
+    ("d1", "yb", 2),
+    ("d1", "xc", 2),
+    ("d1", "yc", 2),
+    ("mma", 7, 2, 2),
+    ("finish", 1, 3),
+    ("d1", "xa", 3),
+    ("d1", "ya", 3),
+    ("mma", 6, 1, 3),
+    ("d1", "xb", 3),
+    ("d1", "yb", 3),
+    ("d1", "xc", 3),
+    ("d1", "yc", 3),
+    ("mma", 7, 2, 3),
+    ("reduce_on",),
+    ("finish", 6, 7, 8),
+    ("reduce", 1),
+)
 
 
 def flip(bit, change):
@@ -49,16 +192,23 @@
     gate_w,
     stat,
     state,
+    late_state,
+    pair_state,
+    y_in,
     aux,
+    pair_aux,
+    y_aux,
     rmem,
     raux,
     local_sem,
+    ready,
     sends,
     x_recv,
     d_recv,
     w_recv,
     g_recv,
     s_recv,
+    y_recv,
     m_recv,
     a_recv,
 ):
@@ -72,12 +222,13 @@
     dv = new_value.shape[2]
     total_heads = input_bias.shape[1]
     key_scale = dk ** (-0.5)
-    per_seq = UNITS // seqs
-    cut = width // (2 * per_seq)
+    cut = width // (2 * PARTS)
+    half = span // 2
     rows_out = dk // count
     zh, zl, y, x = me // 8, (me // 4) % 2, (me // 2) % 2, me % 2
     mine = zl * 2 + x
     inner = zh != zl
+    outer = zh == zl
     bf16, f32 = jnp.bfloat16, jnp.float32
 
     def place(dh, dl, dy, dx):
@@ -110,17 +261,23 @@
     def landed(ref, sem):
         pltpu.make_async_copy(ref, ref, sem).wait()
 
+    to_x, to_y, to_z = place(0, 0, 0, 1), place(0, 0, 1, 0), place(0, 1, 0, 0)
+    to_far, to_mid = place(1, 0, 0, 0), place(1, 1, 0, 0)
     barrier = pltpu.get_barrier_semaphore()
-    for off in range(1, count):
+
+    def tell(sem, sp, tp):
         pl.semaphore_signal(
-            barrier,
-            inc=1,
-            device_id=((me + off) % count, core),
-            device_id_type=pl.DeviceIdType.MESH,
+            sem, inc=1, device_id=(sp, tp), device_id_type=pl.DeviceIdType.MESH
         )
-    pl.semaphore_signal(
-        barrier, inc=1, device_id=(me, 1 - core), device_id_type=pl.DeviceIdType.MESH
-    )
+
+    gate_w[...] = jnp.zeros(gate_w.shape, f32)
+    for peer in (to_x, to_y, to_z):
+        tell(barrier, peer, core)
+    tell(barrier, me, 1 - core)
+
+    @pl.when(inner)
+    def _():
+        tell(barrier, to_mid, core)
 
     def bits(slot):
         return slot // 8, (slot // 4) % 2, (slot // 2) % 2, slot % 2
@@ -137,7 +294,7 @@
     own_x = []
     for s in range(seqs):
         c = pltpu.make_async_copy(
-            prompt.at[s], xb.at[0, pl.ds(s * span, span)], local_sem.at[s]
+            prompt.at[s], xb.at[pl.ds(s * span, span)], local_sem.at[s]
         )
         c.start()
         own_x.append(c)
@@ -148,10 +305,7 @@
     ]
     for c in own_w:
         c.start()
-    pl.semaphore_wait(barrier, count)
-
-    to_x, to_y, to_z = place(0, 0, 0, 1), place(0, 0, 1, 0), place(0, 1, 0, 0)
-    to_far, to_mid = place(1, 0, 0, 0), place(1, 1, 0, 0)
+    pl.semaphore_wait(barrier, 4 + jnp.where(inner, 1, 0))
 
     def w_own(dl, dx, peer, slot, when=None):
         kc, vc = group_cols(dl, dx)
@@ -168,49 +322,79 @@
     def w_wait(slot):
         landed(wb.at[w_rows(slot)], w_recv.at[slot])
 
-    def part(block, unit, owner):
-        s, k = unit // per_seq, unit % per_seq
-        cols = pl.ds(pl.multiple_of((owner * per_seq + k) * cut, cut), cut)
-        return xb.at[block, pl.ds(s * span, span), cols]
-
-    def x_own(block, unit, peer):
-        s, k = unit // per_seq, unit % per_seq
-        cols = pl.ds(pl.multiple_of((core * per_seq + k) * cut, cut), cut)
-        return [
-            remote(
-                prompt.at[s, :, cols],
-                part(block, unit, core),
-                x_recv.at[block, unit],
-                peer,
-                core,
-            )
-        ]
-
-    def x_relay(unit):
-        return [
-            remote(part(2, unit, core), part(3, unit, core), x_recv.at[3, unit], to_x, core)
-        ]
-
-    def x_across(block, unit):
-        own = part(block, unit, core)
-        return [remote(own, own, d_recv.at[block, unit], me, 1 - core)]
-
-    def x_wait(block, unit):
-        landed(part(block, unit, core), x_recv.at[block, unit])
-
-    def d_wait(block, unit):
-        landed(part(block, unit, 1 - core), d_recv.at[block, unit])
-
-    def go_x(block, units):
-        for unit in units:
-            x_wait(block, unit)
-            if block == 2:
-                start(x_relay(unit))
-            start(x_across(block, unit))
-
-    def d_all(block, s):
-        for unit in range(s * per_seq, (s + 1) * per_seq):
-            d_wait(block, unit)
+    def columns(owner, k):
+        return pl.ds(pl.multiple_of((owner * PARTS + k) * cut, cut), cut)
+
+    def rows_of(kind, unit):
+        if kind in ("x1", "x2", "x3"):
+            chunk = {"x1": 2 + unit // PARTS, "x2": 4, "x3": 5}[kind]
+            return chunk * span, span
+        chunk = {"a": 6, "b": 7, "c": 8}[kind[1]]
+        return chunk * span + (half if kind[0] == "y" else 0), half
+
+    def part(kind, unit, owner):
+        low, size = rows_of(kind, unit)
+        return xb.at[pl.ds(low, size), columns(owner, unit % PARTS)]
+
+    def sem(table, kind, unit):
+        return table.at[KINDS.index(kind), unit]
+
+    def x_own(s, low, size, kind, unit, peer, when=None):
+        src = prompt.at[s, pl.ds(low, size), columns(core, unit % PARTS)]
+        copy = remote(src, part(kind, unit, core), sem(x_recv, kind, unit), peer, core, when)
+        start([copy], when)
+
+    def x_pass(kind, there, unit, peer, when=None):
+        copy = remote(
+            part(kind, unit, core),
+            part(there, unit, core),
+            sem(x_recv, there, unit),
+            peer,
+            core,
+            when,
+        )
+        start([copy], when)
+
+    def only(kind):
+        return inner if kind[1] in "bc" else None
+
+    def x_across(kind, unit):
+        own = part(kind, unit, core)
+        when = only(kind)
+        start([remote(own, own, sem(d_recv, kind, unit), me, 1 - core, when)], when)
+
+    def maybe(when, run):
+        if when is None:
+            run()
+        else:
+            pl.when(when)(run)
+
+    def x_wait(kind, unit):
+        maybe(
+            only(kind),
+            lambda: landed(part(kind, unit, core), sem(x_recv, kind, unit)),
+        )
+
+    def d_wait(kind, unit):
+        maybe(
+            only(kind),
+            lambda: landed(part(kind, unit, 1 - core), sem(d_recv, kind, unit)),
+        )
+
+    def go_x(kind, unit):
+        x_wait(kind, unit)
+        if kind == "x2":
+            x_pass("x2", "x3", unit, to_x)
+        if kind == "xa":
+            x_pass("xa", "ya", unit, to_x)
+        if kind == "xc":
+            x_pass("xc", "yc", unit, to_x, inner)
+        if kind == "x1" and unit >= PARTS:
+            k = unit - PARTS
+            src = xb.at[pl.ds(3 * span + half, half), columns(core, k)]
+            dst = part("yb", k, core)
+            start([remote(src, dst, sem(x_recv, "yb", k), to_z, core, outer)], outer)
+        x_across(kind, unit)
 
     def go_w(slot):
         w_wait(slot)
@@ -223,32 +407,20 @@
         w_own(0, 0, to_far, 8),
         w_own(1, 0, to_mid, 12, inner),
     )
-    tokens = [x_own(2, unit, to_z) for unit in range(UNITS)]
-    px = w_own(0, 1, to_x, 1)
+    px, y_own = w_own(0, 1, to_x, 1), w_own(0, 0, to_y, 2)
     kc, vc = group_cols(1, 1)
     px2 = [
         remote(w_key.at[:, kc], pass_w.at[:, :dk], w_recv.at[0], to_x, core),
         remote(w_value.at[:, vc], pass_w.at[:, dk:], w_recv.at[0], to_x, core),
     ]
-    start(px)
-    start(w_own(0, 0, to_y, 2))
-
-    @pl.when(first)
-    def _():
-        start(far)
-        start(near)
-
-    @pl.when(core == 1)
-    def _():
-        start(near)
-        start(far)
-
-    start(px2)
-    start(mid, inner)
-    for unit in range(2):
-        start(tokens[unit])
-    for unit in range(UNITS):
-        start(x_own(1, unit, to_x))
+
+    def greet():
+        @pl.when(inner)
+        def _():
+            tell(ready, to_z, core)
+            tell(ready, to_mid, core)
+
+        pl.semaphore_wait(ready, 1)
 
     w_gate = jnp.concatenate([w_igate[...], w_fgate[...]], axis=0)
     square = iota((total_heads, total_heads), 0) == iota((total_heads, total_heads), 1)
@@ -261,80 +433,84 @@
     spot_head = iota((total_heads, 128), 0) - core * heads
     spot_lane = iota((total_heads, 128), 1)
     local_head = (spot_head >= 0) & (spot_head < heads)
-    for c in own_x:
-        c.wait()
-    packed = jnp.zeros((1, 128), f32)
-    gate_w[0] = jnp.zeros(gate_w.shape[1:], f32)
-    for s in range(seqs):
-        both = lax.dot_general(
-            w_gate,
-            xb[0, s * span : (s + 1) * span],
-            (((1,), (1,)), ((), ())),
-            preferred_element_type=f32,
-        )
-        gate_in = both[:total_heads] + bias_in
-        forget = log_sigmoid(both[total_heads:] + bias_f)
-        level = gate_in + jnp.dot(forget, after, precision=HIGH, preferred_element_type=f32)
-        top = jnp.max(level, axis=1, keepdims=True)
-        total = jnp.sum(forget, axis=1, keepdims=True)
-        part_w = jnp.exp(level - top) * key_scale
-        gate_w[0, s * heads : (s + 1) * heads, :span] = jnp.where(
-            first, part_w[:heads], part_w[heads : 2 * heads]
-        )
-        at = spot_lane - s * heads
-        packed = packed + jnp.sum(
-            jnp.where(local_head & (at == spot_head), total, 0.0)
-            + jnp.where(local_head & (at - seqs * heads == spot_head), top, 0.0),
-            axis=0,
-            keepdims=True,
-        )
-    stat[me] = jnp.broadcast_to(packed, (8, 128))
-    for block in (1, 2, 3):
-        start(
-            [
-                remote(
-                    gate_w.at[0],
-                    gate_w.at[block],
-                    g_recv.at[block],
-                    place(0, block // 2, 0, block % 2),
-                    core,
-                )
-            ]
-        )
-    for off in range(count - 1, 0, -1):
-        peer = place(*bits(off))
-        start([remote(stat.at[me], stat.at[me], s_recv, peer, core)])
-    for c in own_w:
-        c.wait()
-
-    def multiply(blocks, slots, s=None):
-        low, size = (0, seqs * span) if s is None else (s * span, span)
-        pairs = len(slots) // 2
-
-        def choose(i, values):
-            out = jnp.int32(values[0])
-            for k, v in enumerate(values[1:], 1):
-                out = jnp.where(i == k, v, out)
-            return out
+    def gates():
+        for c in own_x:
+            c.wait()
+        packed = jnp.zeros((1, 128), f32)
+        for s in range(seqs):
+            both = lax.dot_general(
+                w_gate,
+                xb[s * span : (s + 1) * span],
+                (((1,), (1,)), ((), ())),
+                preferred_element_type=f32,
+            )
+            gate_in = both[:total_heads] + bias_in
+            forget = log_sigmoid(both[total_heads:] + bias_f)
+            level = gate_in + jnp.dot(forget, after, precision=HIGH, preferred_element_type=f32)
+            top = jnp.max(level, axis=1, keepdims=True)
+            total = jnp.sum(forget, axis=1, keepdims=True)
+            part_w = jnp.exp(level - top) * key_scale
+            gate_w[0, s * heads : (s + 1) * heads, :span] = jnp.where(
+                first, part_w[:heads], part_w[heads : 2 * heads]
+            )
+            at = spot_lane - s * heads
+            packed = packed + jnp.sum(
+                jnp.where(local_head & (at == spot_head), total, 0.0)
+                + jnp.where(local_head & (at - seqs * heads == spot_head), top, 0.0),
+                axis=0,
+                keepdims=True,
+            )
+        stat[me] = jnp.broadcast_to(packed, (8, 128))
+        for c in own_w:
+            c.wait()
+
+    def tell_all():
+        for off in range(count - 1, 0, -1):
+            peer = place(*bits(off))
+            start([remote(stat.at[me], stat.at[me], s_recv, peer, core)])
+        for block, peer in ((1, to_x), (2, to_z), (3, place(0, 1, 0, 1))):
+            start([remote(gate_w.at[0], gate_w.at[block], g_recv.at[block], peer, core)])
+        for block, peer in ((4, to_mid), (5, place(1, 1, 0, 1))):
+            copy = remote(
+                gate_w.at[0], gate_w.at[block], g_recv.at[block], peer, core, inner
+            )
+            start([copy], inner)
+
+    def choose(i, values):
+        out = jnp.int32(values[0])
+        for k, v in enumerate(values[1:], 1):
+            out = jnp.where(i == k, v, out)
+        return out
+
+    def multiply(low, size, slots):
+        width_in = 4 if len(slots) % 4 == 0 else 2
 
         def step(i, carry):
-            block = choose(i // pairs, blocks) if len(blocks) > 1 else blocks[0]
-            at = i % pairs
             out = None
-            for off in range(2):
-                slot = choose(at, slots[off::2]) if pairs > 1 else slots[off]
-                rows = w_rows(slot)
+            for off in range(width_in):
+                rows = w_rows(choose(i, slots[off::width_in]))
                 piece = jnp.dot(
-                    xb[block, pl.ds(low, size), rows], wb[rows], preferred_element_type=f32
+                    xb[pl.ds(low, size), rows], wb[rows], preferred_element_type=f32
                 )
                 out = piece if out is None else out + piece
-            acc[block, pl.ds(low, size)] += out
+            acc[pl.ds(low, size)] += out
             return carry
 
-        lax.fori_loop(0, len(blocks) * pairs, step, 0)
-
-    for block in range(4):
-        acc[block] = jnp.zeros(acc.shape[1:], f32)
+        lax.fori_loop(0, len(slots) // width_in, step, 0)
+
+    def multiply_part(low, size, k):
+        out = None
+        for owner in range(2):
+            cols = slice((owner * PARTS + k) * cut, (owner * PARTS + k + 1) * cut)
+            piece = jnp.dot(xb[low : low + size, cols], wb[cols], preferred_element_type=f32)
+            out = piece if out is None else out + piece
+        acc[low : low + size] += out
+
+    def zero(i, carry):
+        acc[pl.ds(pl.multiple_of(i * span, span), span)] = jnp.zeros((span, dk + dv), f32)
+        return carry
+
+    lax.fori_loop(0, 9, zero, 0)
 
     eye = (iota((span, span), 0) == iota((span, span), 1)).astype(f32)
     here = iota((span, seqs * heads), 1)
@@ -349,9 +525,9 @@
         lift = later[:, : seqs * heads] + table[:, seqs * heads : 2 * seqs * heads]
         highest = jnp.max(lift, axis=0, keepdims=True)
         factor = jnp.exp(lift - highest)
-        for block in range(4):
-            if block:
-                landed(gate_w.at[block], g_recv.at[block])
+        weight[8 * span : 9 * span] = jnp.zeros((span, 128), f32)
+
+        def column(block, s):
             turned = lax.dot_general(
                 eye,
                 gate_w[block][:, :span],
@@ -359,42 +535,69 @@
                 precision=HIGH,
                 preferred_element_type=f32,
             )
-            for s in range(seqs):
-                column = jnp.sum(
-                    jnp.where(here == s * heads + mine, turned, 0.0), axis=1, keepdims=True
-                )
-                hit = (chip == place(0, block // 2, 0, block % 2)) & (lane16 == s * heads + mine)
-                scale = jnp.sum(jnp.where(hit, factor, 0.0), keepdims=True)
-                weight[block, s * span : (s + 1) * span] = jnp.broadcast_to(
-                    column * scale, (span, 128)
-                )
+            dh, pos = (0, block) if block < 4 else (1, 2 + block % 2)
+            lane = s * heads + mine
+            hit = (chip == place(dh, pos // 2, 0, pos % 2)) & (lane16 == lane)
+            scale = jnp.sum(jnp.where(hit, factor, 0.0), keepdims=True)
+            one = jnp.sum(jnp.where(here == lane, turned, 0.0), axis=1, keepdims=True)
+            return jnp.broadcast_to(one * scale, (span, 128))
+
+        for block in range(4):
+            if block:
+                landed(gate_w.at[block], g_recv.at[block])
+            weight[pl.ds((2 * block if block < 2 else 2 + block) * span, span)] = column(block, 0)
+            late = column(block, 1)
+            if block < 2:
+                weight[pl.ds((2 * block + 1) * span, span)] = late
+            else:
+                for chunk in (6, 7):
+                    low = chunk * span + (block - 2) * half
+                    weight[pl.ds(low, half)] = late[(chunk - 6) * half : (chunk - 5) * half]
+
+        @pl.when(inner)
+        def _():
+            for block in (4, 5):
+                landed(gate_w.at[block], g_recv.at[block])
+                low = 8 * span + (block - 4) * half
+                weight[pl.ds(low, half)] = column(block, 1)[half:]
+
         return highest
 
-    def finish(block, s):
-        rows = slice(s * span, (s + 1) * span)
-        to = slice(block * span, (block + 1) * span)
-        keys = acc[block, rows, :dk].astype(bf16).astype(f32)
-        decay[s, to] = (weight[block, rows, 0:1] * keys).astype(bf16)
-        vals[s, to] = acc[block, rows, dk:].astype(bf16)
-
-    ones = jnp.ones((8, 4 * span), bf16)
+    to_chunk = (0, 4, 1, 5, 2, 3, 6, 7, 8)
+
+    def finish(chunk):
+        rows = slice(chunk * span, (chunk + 1) * span)
+        to = slice(to_chunk[chunk] * span, (to_chunk[chunk] + 1) * span)
+        keys = acc[rows, :dk].astype(bf16).astype(f32)
+        decay[to] = (weight[rows, 0:1] * keys).astype(bf16)
+        vals[to] = acc[rows, dk:].astype(bf16)
+
     pick = iota((heads, dk), 0) == mine
 
     def out_rows(chip):
         return pl.ds(pl.multiple_of(chip * rows_out, rows_out), rows_out)
 
     def reduce(s):
-        d = decay[s]
+        span_rows = slice(0, 4 * span) if s == 0 else slice(4 * span, 9 * span)
+        d = decay[span_rows]
+        ones = jnp.ones((8, d.shape[0]), bf16)
         sums = lax.dot_general(
-            d, vals[s], (((0,), (0,)), ((), ())), preferred_element_type=f32
+            d, vals[span_rows], (((0,), (0,)), ((), ())), preferred_element_type=f32
         )
         high = sums.astype(bf16)
-        state[s] = high
-        for off in range(count - 1, 0, -1):
-            peer = place(*bits(off))
-            start(
-                [remote(state.at[s, out_rows(peer)], rmem.at[s, me], m_recv.at[s], peer, core)]
-            )
+        if s == 0:
+            for block in range(count // 2):
+                low = (block // 2) * 2 * rows_out
+                state[block % 2, low : low + 2 * rows_out] = high[
+                    block * 2 * rows_out : (block + 1) * 2 * rows_out
+                ]
+            start([remote(state.at[1 - y], y_in, y_recv.at[0], to_y, core)])
+        else:
+            late_state[...] = high
+            for off in range(count - 1, 0, -1):
+                peer = place(*bits(off))
+                src = late_state.at[out_rows(peer)]
+                start([remote(src, rmem.at[1, me], m_recv.at[1], peer, core)])
         low = (sums - high.astype(f32)).astype(bf16)
         norms = jnp.dot(ones, d, preferred_element_type=f32)
         query = jnp.sum(
@@ -410,82 +613,99 @@
             aux[s, 4 + k : 5 + k] = norms[0:1, k * 128 : (k + 1) * 128]
         dot_norm = jnp.sum(query * norms[0:1], axis=1, keepdims=True)
         aux[s, 6:8] = jnp.broadcast_to(dot_norm, (2, 128))
-        for off in range(count - 1, 0, -1):
-            start([remote(aux.at[s], raux.at[s, me], a_recv.at[s], place(*bits(off)), core)])
-        rmem[s, me] = state[s, out_rows(me)]
-        raux[s, me] = aux[s]
-
-    w_wait(1)
-    start(w_relay(1, to_far, 9))
-    start(w_relay(1, to_y, 3))
-    w_wait(4)
-    start(w_relay(4, to_y, 6))
-    start(w_relay(4, to_far, 12, inner), inner)
-    w_wait(2)
-    multiply([0], [0, 2, 1, 4])
-    landed(pass_w, w_recv.at[0])
-    start([remote(pass_w, wb.at[w_rows(1)], w_recv.at[5], to_z, core)])
-    start(tokens[2])
-    start([remote(pass_w, wb.at[w_rows(1)], w_recv.at[13], to_mid, core, inner)], inner)
-    for unit in range(3, UNITS):
-        start(tokens[unit])
-    go_w(8)
-    w_wait(3)
-    multiply([0], [8, 3])
-    go_x(1, (0, 1))
-    highest = weigh()
-    go_w(5)
-    start(w_relay(5, to_far, 13, inner), inner)
-    w_wait(6)
-    go_x(1, (2, 3))
-    multiply([0], [5, 6])
-    go_w(12)
-    w_wait(10)
-    go_x(2, (0, 1))
-    multiply([0], [12, 10])
-    go_x(1, (4, 5))
-    go_x(2, (2, 3))
-    d_all(1, 0)
-    multiply([1], [0, 2, 1, 4, 8, 3, 5, 6, 12, 10], 0)
-    go_x(1, (6, 7))
-    go_w(9)
-    w_wait(7)
-    multiply([0], [9, 7])
-    go_x(2, (4,))
-    d_all(1, 1)
-    multiply([1], [0, 2, 1, 4, 8, 3, 5, 6, 12, 10], 1)
-    d_all(2, 0)
-    go_x(2, (5,))
-    multiply([2], [0, 2, 1, 4, 8, 3, 5, 6, 12, 10], 0)
-    go_x(3, (0, 1))
-    go_x(2, (6,))
-    go_w(13)
-    w_wait(14)
-    go_x(3, (2, 3))
-    multiply([0, 1], [13, 14])
-    multiply([1], [9, 7])
-    go_x(2, (7,))
-    d_all(3, 0)
-    multiply([3], [0, 2, 1, 4, 8, 3, 5, 6, 12, 10], 0)
-    multiply([2, 3], [9, 7, 13, 14], 0)
-    go_x(3, (4, 5))
-    d_all(2, 1)
-    multiply([2], [0, 2, 1, 4, 8, 3, 5, 6, 12, 10, 9, 7, 13, 14], 1)
-    w_wait(11)
-    w_wait(15)
-    go_x(3, (6,))
-    multiply([0, 1, 2, 3], [11, 15], 0)
-    for block in range(4):
-        finish(block, 0)
-    reduce(0)
-    go_x(3, (7,))
-    multiply([0, 1, 2], [11, 15], 1)
-    for block in range(3):
-        finish(block, 1)
-    d_all(3, 1)
-    multiply([3], [0, 2, 1, 4, 8, 3, 5, 6, 12, 10, 9, 7, 13, 14, 11, 15], 1)
-    finish(3, 1)
-    reduce(1)
+        if s == 0:
+            start([remote(aux.at[0], y_aux, y_recv.at[1], to_y, core)])
+        else:
+            for off in range(count - 1, 0, -1):
+                peer = place(*bits(off))
+                start([remote(aux.at[1], raux.at[1, me], a_recv.at[1], peer, core)])
+            rmem[1, me] = late_state[out_rows(me)]
+            raux[1, me] = aux[1]
+
+    spot8 = (zh * 2 + zl) * 2 + x
+
+    def reduce_on():
+        landed(y_in, y_recv.at[0])
+        pair_state[...] = (state[y].astype(f32) + y_in[...].astype(f32)).astype(bf16)
+        landed(y_aux, y_recv.at[1])
+        pair_aux[...] = aux[0] + y_aux[...]
+        for off in range(count // 2 - 1, 0, -1):
+            dh, dl, dx = off // 4, (off // 2) % 2, off % 2
+            peer = place(dh, dl, 0, dx)
+            spot = (flip(zh, dh) * 2 + flip(zl, dl)) * 2 + flip(x, dx)
+            src = pair_state.at[out_rows(spot)]
+            start([remote(src, rmem.at[0, spot8], m_recv.at[0], peer, core)])
+            start([remote(pair_aux, raux.at[0, spot8], a_recv.at[0], peer, core)])
+        rmem[0, spot8] = pair_state[out_rows(spot8)]
+        raux[0, spot8] = pair_aux[...]
+
+    streams = {"px": px, "px2": px2, "yown": y_own, "near": near}
+    highest = None
+    for name, *arg in SCHEDULE:
+        if name in streams:
+            start(streams[name])
+        elif name == "far":
+            greet()
+            start(far)
+        elif name == "mid":
+            start(mid, inner)
+        elif name == "gates":
+            gates()
+        elif name == "tell_all":
+            tell_all()
+        elif name == "tx":
+            x_own(arg[0] // PARTS, 0, span, "x1", arg[0], to_x)
+        elif name == "tz":
+            x_own(0, 0, span, "x2", arg[0], to_z)
+        elif name == "ta":
+            x_own(1, 0, half, "xa", arg[0], to_z)
+        elif name == "tb":
+            x_own(1, half, half, "xb", arg[0], to_z, outer)
+            x_own(1, half, half, "xc", arg[0], to_mid, inner)
+        elif name == "w":
+            slot = arg[0]
+            w_wait(slot)
+            if slot == 1:
+                start(w_relay(1, to_far, 9))
+            if slot % 4 < 2:
+                start(w_relay(slot, to_y, slot + 2))
+            if slot in (4, 5):
+                start(w_relay(slot, to_far, slot + 8, inner), inner)
+        elif name == "p":
+            landed(pass_w, w_recv.at[0])
+            start([remote(pass_w, wb.at[w_rows(1)], w_recv.at[5], to_z, core)])
+        elif name == "pm":
+            copy = remote(pass_w, wb.at[w_rows(1)], w_recv.at[13], to_mid, core, inner)
+            start([copy], inner)
+        elif name in KINDS:
+            go_x(name, arg[0])
+        elif name == "d":
+            kind, low = arg
+            for unit in range(low, low + PARTS):
+                d_wait(kind, unit)
+        elif name == "mm":
+            low, chunks, slots = arg
+            maybe(
+                inner if low >= 7 else None,
+                lambda: multiply(low * span, chunks * span, slots),
+            )
+        elif name == "d1":
+            d_wait(*arg)
+        elif name == "mma":
+            low, chunks, k = arg
+            maybe(
+                inner if low >= 7 else None,
+                lambda: multiply_part(low * span, chunks * span, k),
+            )
+        elif name == "weigh":
+            highest = weigh()
+        elif name == "finish":
+            for chunk in arg:
+                finish(chunk)
+        elif name == "reduce":
+            reduce(arg[0])
+        elif name == "reduce_on":
+            reduce_on()
 
     def stack(ref):
         return jnp.concatenate([ref[s].astype(f32) for s in range(seqs)], axis=0)
@@ -507,12 +727,16 @@
 
     read_rows, norm_rows, dot_rows = [], [], []
     for s in range(seqs):
-        landed(rmem.at[s, pl.ds(0, count - 1)], m_recv.at[s])
-        landed(raux.at[s, pl.ds(0, count - 1)], a_recv.at[s])
+        peers = count // 2 - 1 if s == 0 else count - 1
+        landed(rmem.at[s, pl.ds(0, peers)], m_recv.at[s])
+        landed(raux.at[s, pl.ds(0, peers)], a_recv.at[s])
         for h in range(heads):
-            srcs = [
-                (a * 2 + h // 2) * 4 + b * 2 + h % 2 for a in range(2) for b in range(2)
-            ]
+            if s == 0:
+                srcs = [(a * 2 + h // 2) * 2 + h % 2 for a in range(2)]
+            else:
+                srcs = [
+                    (a * 2 + h // 2) * 4 + b * 2 + h % 2 for a in range(2) for b in range(2)
+                ]
             mem = rmem[s, srcs[0]].astype(f32)
             both = raux[s, srcs[0]]
             for src in srcs[1:]:
@@ -594,26 +818,33 @@
         in_specs=[hbm, hbm, hbm] + [vmem] * 8,
         out_specs=(vmem, vmem, vmem, vmem),
         scratch_shapes=[
-            pltpu.VMEM((4, rows, width), jnp.bfloat16),
+            pltpu.VMEM((9 * span, width), jnp.bfloat16),
             pltpu.VMEM((width, dk + dv), jnp.bfloat16),
             pltpu.VMEM((depth, dk + dv), jnp.bfloat16),
-            pltpu.VMEM((4, rows, dk + dv), jnp.float32),
-            pltpu.VMEM((seqs, 4 * span, dk), jnp.bfloat16),
-            pltpu.VMEM((seqs, 4 * span, dv), jnp.bfloat16),
-            pltpu.VMEM((4, rows, 128), jnp.float32),
-            pltpu.VMEM((4, 8, 256), jnp.float32),
+            pltpu.VMEM((9 * span, dk + dv), jnp.float32),
+            pltpu.VMEM((9 * span, dk), jnp.bfloat16),
+            pltpu.VMEM((9 * span, dv), jnp.bfloat16),
+            pltpu.VMEM((9 * span, 128), jnp.float32),
+            pltpu.VMEM((6, 8, 256), jnp.float32),
             pltpu.VMEM((count, 8, 128), jnp.float32),
-            pltpu.VMEM((seqs, dk, dv), jnp.bfloat16),
+            pltpu.VMEM((2, dk // 2, dv), jnp.bfloat16),
+            pltpu.VMEM((dk, dv), jnp.bfloat16),
+            pltpu.VMEM((dk // 2, dv), jnp.bfloat16),
+            pltpu.VMEM((dk // 2, dv), jnp.bfloat16),
             pltpu.VMEM((seqs, 8, 128), jnp.float32),
+            pltpu.VMEM((8, 128), jnp.float32),
+            pltpu.VMEM((8, 128), jnp.float32),
             pltpu.VMEM((seqs, count, dk // count, dv), jnp.bfloat16),
             pltpu.VMEM((seqs, count, 8, 128), jnp.float32),
             dma((4,)),
+            pltpu.SemaphoreType.REGULAR,
             dma((SENDS,)),
-            dma((4, UNITS)),
-            dma((4, UNITS)),
+            dma((len(KINDS), 2 * PARTS)),
+            dma((len(KINDS), 2 * PARTS)),
             dma((16,)),
-            dma((4,)),
+            dma((6,)),
             dma,
+            dma((2,)),
             dma((seqs,)),
             dma((seqs,)),
         ],

time: 121 us -> 118 us (0.975)
  Pallas kernels: 120 us -> 118 us
    pallas_call x1, Pallas kernels: 118 us -> 116 us  [by_head(): pl.pallas_call(kernel, out_shape=(jax.ShapeDtypeStruct((seqs, heads, dk /...]
where the time goes in v2:
time: 118 us
  Pallas kernels  118 us (100%)
    pallas_call x1, Pallas kernels, by_head(): pl.pallas_call(kernel, out_shape=(jax.ShapeDtypeStruct((seqs, heads, dk /...  116 us

profile of v2, /device:TPU:0, one launch (start us, length us, event | category | flops | bytes accessed | tf_op | source)
XLA Modules:
  0.0 118.2 jit_solution(3002828418958317035)
XLA Ops:
  0.6 116.0 %shard_map.138 = (bf16[2,4,16,512]{3,2,1,0:T(8,128)(2,1)}, f32[8,16]{1,0:T(8,128)}, f32[8,1]{1,0:T(8,128)}, bf16[8,512]{1,0:T(8,128)(2,1)}) custom-call(bf16[2,192,4096]{2,1,0:T(8,128)(2,1)} %prompt.1, bf16[256,1024]{1,0:T(8,128)(2,1)} %w_key.1, bf16[256,2048]{1,0:T(8,128)(2,1)} %w_value.1, bf16[8,4096]{1,0:T(8,128)(2,1)} %bitcast.4, ...), custom_call_target="tpu_custom_call" | custom-call | tf_op jit(solution)/shard_map/pallas_call | solution.py:810
  116.7 1.6 %shard_map.139 = (bf16[2,4,16,512]{3,2,1,0:T(8,128)(2,1)}, f32[2,4,16]{2,1,0:T(4,128)}, f32[2,4]{1,0:T(2,128)}, bf16[2,4,512]{2,1,0:T(4,128)(2,1)}) custom-call(bf16[2,4,16,512]{3,2,1,0:T(8,128)(2,1)} %get-tuple-element.8.memory, f32[8,16]{1,0:T(8,128)} %get-tuple-element.9.norm, f32[8,1]{1,0:T(8,128)} %get-tuple-element.10.top, ...), custom_call_target="tpu_custom_call" | custom-call | tf_op jit(solution)/shard_map/pallas_call | solution.py:867

commit v3 on v2

--- a/solution.py
+++ b/solution.py
@@ -12,102 +12,101 @@
 SENDS = 180
 SCHEDULE = (
     ("far",),
-    ("px2",),
     ("tx", 0),
-    ("mid",),
-    ("tz", 0),
-    ("near",),
     ("px",),
     ("tx", 1),
+    ("near",),
+    ("x1", 0),
     ("yown",),
+    ("tz", 0),
+    ("tz", 1),
+    ("w", 1),
+    ("px2",),
+    ("w", 8),
+    ("gates",),
+    ("x1", 1),
+    ("mid",),
+    ("tx", 2),
+    ("tz", 2),
+    ("tx", 3),
+    ("p",),
+    ("tx", 4),
+    ("w", 4),
+    ("tz", 3),
     ("x2", 0),
-    ("tx", 2),
-    ("w", 8),
+    ("w", 9),
+    ("w", 3),
     ("tb", 0),
-    ("tx", 3),
-    ("tz", 1),
-    ("p",),
-    ("w", 4),
-    ("w", 1),
-    ("tz", 2),
+    ("tx", 5),
+    ("ta", 0),
+    ("x1", 2),
+    ("tx", 6),
+    ("x2", 1),
+    ("x1", 3),
+    ("ta", 1),
+    ("w", 2),
+    ("x3", 0),
+    ("tx", 7),
+    ("w", 12),
+    ("x1", 4),
     ("pm",),
-    ("tx", 4),
-    ("w", 12),
-    ("tx", 5),
-    ("x1", 0),
-    ("x1", 1),
-    ("x2", 1),
-    ("tx", 6),
-    ("tz", 3),
-    ("w", 2),
+    ("x3", 1),
+    ("w", 10),
+    ("x1", 5),
+    ("mm", 0, 2, (1, 8, 0, 4)),
+    ("x2", 2),
+    ("x1", 6),
     ("w", 5),
-    ("x1", 2),
-    ("xb", 0),
-    ("x3", 0),
-    ("x1", 3),
-    ("gates",),
-    ("w", 3),
-    ("x1", 4),
-    ("x1", 5),
-    ("ta", 0),
+    ("x2", 3),
     ("tb", 1),
-    ("ta", 1),
-    ("tx", 7),
-    ("x1", 6),
-    ("mm", 0, 2, (8, 4, 1, 12)),
-    ("x2", 2),
-    ("w", 10),
-    ("x3", 1),
-    ("mm", 0, 2, (2, 5, 0, 3)),
+    ("w", 14),
+    ("xc", 0),
     ("ta", 2),
-    ("yb", 0),
-    ("w", 9),
+    ("tell_all",),
+    ("w", 11),
+    ("x3", 2),
+    ("tb", 2),
+    ("w", 13),
+    ("ta", 3),
     ("x1", 7),
-    ("x2", 3),
+    ("xa", 0),
     ("d", "x1", 0),
     ("d", "x1", 4),
-    ("mm", 2, 2, (8, 4, 1, 12)),
-    ("yb", 1),
-    ("w", 6),
-    ("mm", 2, 2, (2, 5, 0, 3)),
-    ("xc", 0),
-    ("w", 14),
-    ("tell_all",),
-    ("x3", 2),
-    ("ta", 3),
-    ("w", 13),
-    ("tb", 2),
-    ("xa", 0),
+    ("mm", 2, 2, (1, 8, 0, 4)),
+    ("xb", 0),
     ("xa", 1),
+    ("tb", 3),
+    ("mm", 0, 2, (9, 3, 2, 12)),
     ("x3", 3),
-    ("tb", 3),
+    ("mm", 2, 2, (9, 3, 2, 12, 10, 5, 14, 11)),
+    ("mm", 0, 2, (10, 5, 14, 11)),
     ("d", "x2", 0),
     ("d", "x3", 0),
-    ("mm", 4, 2, (8, 4, 1, 12)),
-    ("mm", 2, 2, (10, 9, 6, 14)),
-    ("mm", 4, 2, (2, 5, 0, 3)),
+    ("mm", 4, 2, (1, 8, 0, 4, 9, 3, 2, 12)),
+    ("xc", 1),
+    ("yc", 0),
+    ("mm", 4, 2, (10, 5, 14, 11)),
+    ("w", 7),
+    ("yb", 0),
+    ("ya", 0),
+    ("w", 6),
+    ("yb", 1),
     ("xa", 2),
-    ("mm", 0, 2, (10, 9, 6, 14)),
-    ("yb", 2),
-    ("yc", 0),
-    ("yb", 3),
-    ("mm", 4, 2, (10, 9, 6, 14)),
-    ("xc", 1),
-    ("w", 7),
     ("xc", 2),
-    ("ya", 0),
+    ("weigh",),
+    ("xb", 1),
+    ("xc", 3),
     ("xa", 3),
-    ("weigh",),
-    ("xc", 3),
     ("ya", 1),
-    ("w", 11),
-    ("xb", 1),
+    ("xb", 2),
     ("w", 15),
-    ("mm", 4, 2, (13, 7, 11, 15)),
-    ("mm", 0, 2, (13, 7, 11, 15)),
-    ("mm", 2, 2, (13, 7, 11, 15)),
+    ("mm", 4, 2, (13, 7, 6, 15)),
+    ("mm", 0, 2, (13, 7, 6, 15)),
+    ("mm", 2, 2, (13, 7, 6, 15)),
     ("finish", 0, 2, 4, 5),
     ("reduce", 0),
+    ("yc", 1),
+    ("ya", 2),
     ("d1", "xa", 0),
     ("d1", "ya", 0),
     ("mma", 6, 1, 0),
@@ -116,7 +115,8 @@
     ("d1", "xc", 0),
     ("d1", "yc", 0),
     ("mma", 7, 2, 0),
-    ("yc", 1),
+    ("ya", 3),
+    ("yc", 2),
     ("d1", "xa", 1),
     ("d1", "ya", 1),
     ("mma", 6, 1, 1),
@@ -125,10 +125,7 @@
     ("d1", "xc", 1),
     ("d1", "yc", 1),
     ("mma", 7, 2, 1),
-    ("ya", 2),
-    ("yc", 2),
-    ("xb", 2),
-    ("ya", 3),
+    ("yb", 2),
     ("xb", 3),
     ("yc", 3),
     ("d1", "xa", 2),
@@ -139,6 +136,8 @@
     ("d1", "xc", 2),
     ("d1", "yc", 2),
     ("mma", 7, 2, 2),
+    ("reduce_on",),
+    ("yb", 3),
     ("finish", 1, 3),
     ("d1", "xa", 3),
     ("d1", "ya", 3),
@@ -148,7 +147,6 @@
     ("d1", "xc", 3),
     ("d1", "yc", 3),
     ("mma", 7, 2, 3),
-    ("reduce_on",),
     ("finish", 6, 7, 8),
     ("reduce", 1),
 )
@@ -386,7 +384,7 @@
         if kind == "x2":
             x_pass("x2", "x3", unit, to_x)
         if kind == "xa":
-            x_pass("xa", "ya", unit, to_x)
+            x_pass("xa", "ya", unit, to_x, outer if unit >= PARTS // 2 else None)
         if kind == "xc":
             x_pass("xc", "yc", unit, to_x, inner)
         if kind == "x1" and unit >= PARTS:
@@ -394,6 +392,10 @@
             src = xb.at[pl.ds(3 * span + half, half), columns(core, k)]
             dst = part("yb", k, core)
             start([remote(src, dst, sem(x_recv, "yb", k), to_z, core, outer)], outer)
+            if k >= PARTS // 2:
+                src = xb.at[pl.ds(3 * span, half), columns(core, k)]
+                dst = part("ya", k, core)
+                start([remote(src, dst, sem(x_recv, "ya", k), to_z, core, outer)], outer)
         x_across(kind, unit)
 
     def go_w(slot):

time: 118 us -> 116 us (0.983)
  Pallas kernels: 118 us -> 115 us
    pallas_call x1, Pallas kernels: 116 us -> 114 us  [by_head(): pl.pallas_call(kernel, out_shape=(jax.ShapeDtypeStruct((seqs, heads, dk /...]
where the time goes in v3:
time: 116 us
  Pallas kernels  115 us (99%)
    pallas_call x1, Pallas kernels, by_head(): pl.pallas_call(kernel, out_shape=(jax.ShapeDtypeStruct((seqs, heads, dk /...  114 us

profile of v3, /device:TPU:0, one launch (start us, length us, event | category | flops | bytes accessed | tf_op | source)
XLA Modules:
  0.0 116.1 jit_solution(17556499471529712723)
XLA Ops:
  0.6 113.9 %shard_map.138 = (bf16[2,4,16,512]{3,2,1,0:T(8,128)(2,1)}, f32[8,16]{1,0:T(8,128)}, f32[8,1]{1,0:T(8,128)}, bf16[8,512]{1,0:T(8,128)(2,1)}) custom-call(bf16[2,192,4096]{2,1,0:T(8,128)(2,1)} %prompt.1, bf16[256,1024]{1,0:T(8,128)(2,1)} %w_key.1, bf16[256,2048]{1,0:T(8,128)(2,1)} %w_value.1, bf16[8,4096]{1,0:T(8,128)(2,1)} %bitcast.4, ...), custom_call_target="tpu_custom_call" | custom-call | tf_op jit(solution)/shard_map/pallas_call | solution.py:812
  114.5 1.6 %shard_map.139 = (bf16[2,4,16,512]{3,2,1,0:T(8,128)(2,1)}, f32[2,4,16]{2,1,0:T(4,128)}, f32[2,4]{1,0:T(2,128)}, bf16[2,4,512]{2,1,0:T(4,128)(2,1)}) custom-call(bf16[2,4,16,512]{3,2,1,0:T(8,128)(2,1)} %get-tuple-element.8.memory, f32[8,16]{1,0:T(8,128)} %get-tuple-element.9.norm, f32[8,1]{1,0:T(8,128)} %get-tuple-element.10.top, ...), custom_call_target="tpu_custom_call" | custom-call | tf_op jit(solution)/shard_map/pallas_call | solution.py:869

commit v4 on v3

--- a/solution.py
+++ b/solution.py
@@ -9,104 +9,125 @@
 HIGH = lax.Precision.HIGHEST
 PARTS = 4
 KINDS = ("x1", "x2", "x3", "xa", "ya", "xb", "yb", "xc", "yc")
-SENDS = 180
+SENDS = 212
 SCHEDULE = (
-    ("far",),
+    ("far", 0),
     ("tx", 0),
-    ("px",),
+    ("px", 0),
+    ("near", 0),
     ("tx", 1),
-    ("near",),
+    ("px2", 0),
+    ("mid", 0),
+    ("tz", 0),
+    ("yown", 0),
+    ("near", 1),
+    ("px", 1),
+    ("tb", 0),
+    ("yown", 1),
+    ("w", 4, 0),
+    ("px2", 1),
+    ("w", 1, 0),
     ("x1", 0),
-    ("yown",),
-    ("tz", 0),
+    ("p", 0),
+    ("w", 8, 0),
+    ("x2", 0),
+    ("tx", 2),
+    ("mid", 1),
+    ("w", 1, 1),
+    ("gates",),
+    ("w", 4, 1),
+    ("tx", 3),
+    ("w", 12, 0),
+    ("tx", 4),
+    ("pm", 0),
     ("tz", 1),
-    ("w", 1),
-    ("px2",),
-    ("w", 8),
-    ("gates",),
+    ("p", 1),
+    ("w", 5, 0),
+    ("x2", 1),
     ("x1", 1),
-    ("mid",),
-    ("tx", 2),
+    ("w", 2, 0),
+    ("w", 9, 0),
     ("tz", 2),
-    ("tx", 3),
-    ("p",),
-    ("tx", 4),
-    ("w", 4),
+    ("pm", 1),
+    ("tx", 5),
     ("tz", 3),
-    ("x2", 0),
-    ("w", 9),
-    ("w", 3),
-    ("tb", 0),
-    ("tx", 5),
+    ("w", 5, 1),
+    ("far", 1),
+    ("mm", 0, 2, (1, 0, 4, 5)),
+    ("x1", 2),
+    ("x1", 3),
+    ("w", 9, 1),
+    ("x1", 4),
+    ("tx", 6),
+    ("x2", 2),
+    ("w", 7, 0),
     ("ta", 0),
-    ("x1", 2),
-    ("tx", 6),
-    ("x2", 1),
-    ("x1", 3),
+    ("w", 3, 0),
+    ("x3", 0),
+    ("w", 12, 1),
+    ("w", 7, 1),
+    ("tx", 7),
+    ("w", 14, 0),
+    ("w", 6, 1),
+    ("x1", 5),
+    ("w", 10, 0),
+    ("tell_all",),
     ("ta", 1),
-    ("w", 2),
-    ("x3", 0),
-    ("tx", 7),
-    ("w", 12),
-    ("x1", 4),
-    ("pm",),
+    ("xb", 0),
+    ("ta", 2),
+    ("x2", 3),
+    ("w", 11, 0),
+    ("x1", 6),
+    ("w", 6, 0),
+    ("w", 2, 1),
+    ("ta", 3),
+    ("w", 3, 1),
+    ("w", 13, 0),
+    ("yb", 0),
+    ("w", 11, 1),
+    ("mm", 0, 2, (9, 12, 7, 6)),
+    ("tb", 1),
+    ("w", 13, 1),
+    ("yb", 1),
+    ("xc", 0),
+    ("mm", 0, 2, (2, 3, 11, 13)),
+    ("tb", 2),
+    ("x1", 7),
     ("x3", 1),
-    ("w", 10),
-    ("x1", 5),
-    ("mm", 0, 2, (1, 8, 0, 4)),
-    ("x2", 2),
-    ("x1", 6),
-    ("w", 5),
-    ("x2", 3),
-    ("tb", 1),
-    ("w", 14),
-    ("xc", 0),
-    ("ta", 2),
-    ("tell_all",),
-    ("w", 11),
-    ("x3", 2),
-    ("tb", 2),
-    ("w", 13),
-    ("ta", 3),
-    ("x1", 7),
+    ("w", 15, 0),
+    ("w", 8, 1),
+    ("w", 14, 1),
     ("xa", 0),
     ("d", "x1", 0),
     ("d", "x1", 4),
-    ("mm", 2, 2, (1, 8, 0, 4)),
-    ("xb", 0),
+    ("mm", 2, 2, (1, 0, 4, 5, 9, 12, 7, 6)),
+    ("x3", 2),
+    ("yb", 2),
+    ("mm", 2, 2, (2, 3, 11, 13)),
+    ("tb", 3),
+    ("x3", 3),
     ("xa", 1),
-    ("tb", 3),
-    ("mm", 0, 2, (9, 3, 2, 12)),
-    ("x3", 3),
-    ("mm", 2, 2, (9, 3, 2, 12, 10, 5, 14, 11)),
-    ("mm", 0, 2, (10, 5, 14, 11)),
+    ("weigh",),
+    ("xa", 2),
     ("d", "x2", 0),
     ("d", "x3", 0),
-    ("mm", 4, 2, (1, 8, 0, 4, 9, 3, 2, 12)),
+    ("mm", 4, 2, (1, 0, 4, 5, 9, 12, 7, 6, 2, 3, 11, 13)),
     ("xc", 1),
-    ("yc", 0),
-    ("mm", 4, 2, (10, 5, 14, 11)),
-    ("w", 7),
-    ("yb", 0),
-    ("ya", 0),
-    ("w", 6),
-    ("yb", 1),
-    ("xa", 2),
+    ("xa", 3),
+    ("w", 15, 1),
+    ("w", 10, 1),
+    ("mm", 2, 2, (8, 14, 15, 10)),
+    ("mm", 0, 2, (8, 14, 15, 10)),
     ("xc", 2),
-    ("weigh",),
-    ("xb", 1),
-    ("xc", 3),
-    ("xa", 3),
-    ("ya", 1),
-    ("xb", 2),
-    ("w", 15),
-    ("mm", 4, 2, (13, 7, 6, 15)),
-    ("mm", 0, 2, (13, 7, 6, 15)),
-    ("mm", 2, 2, (13, 7, 6, 15)),
+    ("mm", 4, 2, (8, 14, 15, 10)),
     ("finish", 0, 2, 4, 5),
     ("reduce", 0),
+    ("xb", 1),
+    ("ya", 0),
+    ("yc", 0),
+    ("xc", 3),
+    ("yb", 3),
     ("yc", 1),
-    ("ya", 2),
     ("d1", "xa", 0),
     ("d1", "ya", 0),
     ("mma", 6, 1, 0),
@@ -115,8 +136,7 @@
     ("d1", "xc", 0),
     ("d1", "yc", 0),
     ("mma", 7, 2, 0),
-    ("ya", 3),
-    ("yc", 2),
+    ("ya", 1),
     ("d1", "xa", 1),
     ("d1", "ya", 1),
     ("mma", 6, 1, 1),
@@ -125,9 +145,13 @@
     ("d1", "xc", 1),
     ("d1", "yc", 1),
     ("mma", 7, 2, 1),
-    ("yb", 2),
+    ("ya", 2),
+    ("ya", 3),
+    ("xb", 2),
+    ("yc", 2),
+    ("yc", 3),
+    ("reduce_on",),
     ("xb", 3),
-    ("yc", 3),
     ("d1", "xa", 2),
     ("d1", "ya", 2),
     ("mma", 6, 1, 2),
@@ -136,8 +160,6 @@
     ("d1", "xc", 2),
     ("d1", "yc", 2),
     ("mma", 7, 2, 2),
-    ("reduce_on",),
-    ("yb", 3),
     ("finish", 1, 3),
     ("d1", "xa", 3),
     ("d1", "ya", 3),
@@ -305,20 +327,33 @@
         c.start()
     pl.semaphore_wait(barrier, 4 + jnp.where(inner, 1, 0))
 
-    def w_own(dl, dx, peer, slot, when=None):
+    piece = depth // 2
+
+    def w_part(slot, k):
+        low = place(*bits(slot)) * depth + k * piece
+        return pl.ds(pl.multiple_of(low, piece), piece)
+
+    def w_sem(slot, k):
+        return w_recv.at[2 * slot + k]
+
+    def w_own(dl, dx, peer, slot, k, when=None):
         kc, vc = group_cols(dl, dx)
-        rows = w_rows(0)
-        return [
-            remote(w_key.at[:, kc], wb.at[rows, :dk], w_recv.at[slot], peer, core, when),
-            remote(w_value.at[:, vc], wb.at[rows, dk:], w_recv.at[slot], peer, core, when),
+        src, dst = pl.ds(k * piece, piece), w_part(0, k)
+        copies = [
+            remote(w_key.at[src, kc], wb.at[dst, :dk], w_sem(slot, k), peer, core, when),
+            remote(w_value.at[src, vc], wb.at[dst, dk:], w_sem(slot, k), peer, core, when),
         ]
-
-    def w_relay(slot, peer, there, when=None):
-        rows = w_rows(slot)
-        return [remote(wb.at[rows], wb.at[rows], w_recv.at[there], peer, core, when)]
-
-    def w_wait(slot):
-        landed(wb.at[w_rows(slot)], w_recv.at[slot])
+        start(copies, when)
+
+    def w_relay(slot, k, peer, there, when=None):
+        rows = w_part(slot, k)
+        start([remote(wb.at[rows], wb.at[rows], w_sem(there, k), peer, core, when)], when)
+
+    def w_wait(slot, k):
+        landed(wb.at[w_part(slot, k)], w_sem(slot, k))
+
+    def pass_rows(k):
+        return pass_w.at[pl.ds(k * piece, piece)]
 
     def columns(owner, k):
         return pl.ds(pl.multiple_of((owner * PARTS + k) * cut, cut), cut)
@@ -398,23 +433,17 @@
                 start([remote(src, dst, sem(x_recv, "ya", k), to_z, core, outer)], outer)
         x_across(kind, unit)
 
-    def go_w(slot):
-        w_wait(slot)
-        start(w_relay(slot, to_y, slot + 2))
-
     first = core == 0
 
-    near, far, mid = (
-        w_own(1, 0, to_z, 4),
-        w_own(0, 0, to_far, 8),
-        w_own(1, 0, to_mid, 12, inner),
-    )
-    px, y_own = w_own(0, 1, to_x, 1), w_own(0, 0, to_y, 2)
-    kc, vc = group_cols(1, 1)
-    px2 = [
-        remote(w_key.at[:, kc], pass_w.at[:, :dk], w_recv.at[0], to_x, core),
-        remote(w_value.at[:, vc], pass_w.at[:, dk:], w_recv.at[0], to_x, core),
-    ]
+    def px2(k):
+        kc, vc = group_cols(1, 1)
+        src, dst = pl.ds(k * piece, piece), pass_rows(k)
+        start(
+            [
+                remote(w_key.at[src, kc], dst.at[:, :dk], w_sem(0, k), to_x, core),
+                remote(w_value.at[src, vc], dst.at[:, dk:], w_sem(0, k), to_x, core),
+            ]
+        )
 
     def greet():
         @pl.when(inner)
@@ -641,16 +670,21 @@
         rmem[0, spot8] = pair_state[out_rows(spot8)]
         raux[0, spot8] = pair_aux[...]
 
-    streams = {"px": px, "px2": px2, "yown": y_own, "near": near}
+    streams = {"px": (0, 1, to_x, 1), "yown": (0, 0, to_y, 2), "near": (1, 0, to_z, 4)}
+    greeted = False
     highest = None
     for name, *arg in SCHEDULE:
         if name in streams:
-            start(streams[name])
+            w_own(*streams[name], arg[0])
+        elif name == "px2":
+            px2(arg[0])
         elif name == "far":
-            greet()
-            start(far)
+            if not greeted:
+                greet()
+            greeted = True
+            w_own(0, 0, to_far, 8, arg[0])
         elif name == "mid":
-            start(mid, inner)
+            w_own(1, 0, to_mid, 12, arg[0], inner)
         elif name == "gates":
             gates()
         elif name == "tell_all":
@@ -665,20 +699,23 @@
             x_own(1, half, half, "xb", arg[0], to_z, outer)
             x_own(1, half, half, "xc", arg[0], to_mid, inner)
         elif name == "w":
-            slot = arg[0]
-            w_wait(slot)
+            slot, k = arg
+            w_wait(slot, k)
             if slot == 1:
-                start(w_relay(1, to_far, 9))
+                w_relay(1, k, to_far, 9)
             if slot % 4 < 2:
-                start(w_relay(slot, to_y, slot + 2))
+                w_relay(slot, k, to_y, slot + 2)
             if slot in (4, 5):
-                start(w_relay(slot, to_far, slot + 8, inner), inner)
+                w_relay(slot, k, to_far, slot + 8, inner)
         elif name == "p":
-            landed(pass_w, w_recv.at[0])
-            start([remote(pass_w, wb.at[w_rows(1)], w_recv.at[5], to_z, core)])
+            k = arg[0]
+            landed(pass_rows(k), w_sem(0, k))
+            dst = wb.at[w_part(1, k)]
+            start([remote(pass_rows(k), dst, w_sem(5, k), to_z, core)])
         elif name == "pm":
-            copy = remote(pass_w, wb.at[w_rows(1)], w_recv.at[13], to_mid, core, inner)
-            start([copy], inner)
+            k = arg[0]
+            dst = wb.at[w_part(1, k)]
+            start([remote(pass_rows(k), dst, w_sem(13, k), to_mid, core, inner)], inner)
         elif name in KINDS:
             go_x(name, arg[0])
         elif name == "d":
@@ -843,7 +880,7 @@
             dma((SENDS,)),
             dma((len(KINDS), 2 * PARTS)),
             dma((len(KINDS), 2 * PARTS)),
-            dma((16,)),
+            dma((32,)),
             dma((6,)),
             dma,
             dma((2,)),

time: 116 us -> 115 us (level)
  no operation moved by 1% of the time
where the time goes in v4:
time: 115 us
  Pallas kernels  114 us (99%)
    pallas_call x1, Pallas kernels, by_head(): pl.pallas_call(kernel, out_shape=(jax.ShapeDtypeStruct((seqs, heads, dk /...  113 us

profile of v4, /device:TPU:0, one launch (start us, length us, event | category | flops | bytes accessed | tf_op | source)
XLA Modules:
  0.0 115.1 jit_solution(13849007112934542085)
XLA Ops:
  0.6 112.9 %shard_map.138 = (bf16[2,4,16,512]{3,2,1,0:T(8,128)(2,1)}, f32[8,16]{1,0:T(8,128)}, f32[8,1]{1,0:T(8,128)}, bf16[8,512]{1,0:T(8,128)(2,1)}) custom-call(bf16[2,192,4096]{2,1,0:T(8,128)(2,1)} %prompt.1, bf16[256,1024]{1,0:T(8,128)(2,1)} %w_key.1, bf16[256,2048]{1,0:T(8,128)(2,1)} %w_value.1, bf16[8,4096]{1,0:T(8,128)(2,1)} %bitcast.4, ...), custom_call_target="tpu_custom_call" | custom-call | tf_op jit(solution)/shard_map/pallas_call | solution.py:849
  113.5 1.6 %shard_map.139 = (bf16[2,4,16,512]{3,2,1,0:T(8,128)(2,1)}, f32[2,4,16]{2,1,0:T(4,128)}, f32[2,4]{1,0:T(2,128)}, bf16[2,4,512]{2,1,0:T(4,128)(2,1)}) custom-call(bf16[2,4,16,512]{3,2,1,0:T(8,128)(2,1)} %get-tuple-element.8.memory, f32[8,16]{1,0:T(8,128)} %get-tuple-element.9.norm, f32[8,1]{1,0:T(8,128)} %get-tuple-element.10.top, ...), custom_call_target="tpu_custom_call" | custom-call | tf_op jit(solution)/shard_map/pallas_call | solution.py:906
